TPU v7x, 32 devices: a whole 2x2x4 slice. The times are simulated.
32 devices in a mesh: sp: 16 (over z, y, x), tp: 2 (over core).
Axes of the slice: x: 2, y: 2, z: 4, core: 2. Of those that a mesh axis runs over, the one named last changes fastest.
Arguments:
- tokens: bfloat16 [4096, 2048], P('sp'), may hold values from -6 to 6
- input_norm_gain: float32 [2048], replicated, may hold values from 0.1 to 1.9
- query_matrix: bfloat16 [2048, 1024], P('sp', 'tp'), may hold values from -0.125 to 0.125
- key_matrix: bfloat16 [2048, 1024], P('sp', 'tp'), may hold values from -0.125 to 0.125
- value_matrix: bfloat16 [2048, 1024], P('sp', 'tp'), may hold values from -0.125 to 0.125
- convolution_value_matrix: bfloat16 [2048, 2048], P('sp', 'tp'), may hold values from -0.125 to 0.125
- convolution_gate_matrix: bfloat16 [2048, 2048], P('sp', 'tp'), may hold values from -0.125 to 0.125
- decay_offset_channel: float32 [1024], P('tp'), may hold values from -16 to -2
- decay_first_matrix: bfloat16 [2048, 128], replicated, may hold values from -0.125 to 0.125
- decay_second_matrix: bfloat16 [128, 1024], P(None, 'tp'), may hold values from -0.59765625 to 0.59765625
- learning_rate_offset: float32 [1024], P('tp'), may hold values from -9 to 1
- learning_rate_first_matrix: bfloat16 [2048, 128], replicated, may hold values from -0.125 to 0.125
- learning_rate_second_matrix: bfloat16 [128, 1024], P(None, 'tp'), may hold values from -0.5 to 0.5
- forgetting_rate_factor: float32 [4096, 16], P('sp', 'tp'), may hold values from 0.39 to 2.53
- state_retention_share: float32 [4096, 16], P('sp', 'tp'), may hold values from 0.12 to 1
- per_head_norm_gain: float32 [1024], P('tp'), may hold values from 0.1 to 1.9
- convolution_filter_taps: float32 [31, 2048], P(None, 'tp'), may hold values from -81 to 81
- convolution_channel_gain: float32 [2048], P('tp'), may hold values from 0.1 to 1.9
- attention_output_matrix: bfloat16 [2048, 1024], P('sp', 'tp'), may hold values from -0.109375 to 0.109375
- convolution_output_matrix: bfloat16 [2048, 2048], P('sp', 'tp'), may hold values from -0.109375 to 0.109375
Outputs:
- mixed: bfloat16 [4096, 2048], P('sp')
All inputs are finite; a program needn't handle non-finite values.
Results may differ from a plain program's by a relative error of at most 0.014.
Values may be sent and summed in bfloat16 or wider, within the bound.
A program may use at most 128 MiB of HBM per device.

v0:
```python
import math

import jax
import jax.numpy as jnp
from jax import lax
from jax.sharding import PartitionSpec as P

CONV_CH = 2048


HIGHEST = lax.Precision.HIGHEST
RMS_EPSILON = 1e-06
GROUP_EPSILON = 0.00064
LAYER_EPSILON = 1e-05
UNIT_EPSILON = 1e-06


def entering(x, axis, combine, identity):
    count, place = (lax.axis_size(axis), lax.axis_index(axis))
    everything = jax.tree.map(lambda part: lax.all_gather(part, axis), x)
    start = jax.tree.map(
        lambda part, zero: jnp.broadcast_to(jnp.asarray(zero, part.dtype), part.shape), x, identity
    )

    def hop(k, before):
        reached = k < place
        new = combine(before, jax.tree.map(lambda part: part[k], everything))
        return jax.tree.map(lambda a, b: jnp.where(reached, a, b), new, before)

    return lax.fori_loop(0, count, hop, start)


def from_behind(value, axis, steps):
    count = lax.axis_size(axis)
    initial, last = (max(0, -steps), min(count, count - steps))
    return lax.ppermute(value, axis, [(source, source + steps) for source in range(initial, last)])


def exact_mul(form, left, right):
    return jnp.einsum(form, left, right, precision=HIGHEST)


def chain_pair(earlier, later):
    return (
        exact_mul("...cd,...de->...ce", earlier[0], later[0]),
        exact_mul("...vd,...de->...ve", earlier[1], later[0]) + later[1],
    )


def split_blocks(values, block_count, block_len):
    return values.reshape((block_count, block_len) + values.shape[1:]).transpose(0, 2, 1, 3)


def block_update(carry, inputs):
    phi_sofar, psi_sofar = carry
    query_blk, logdec_blk, key_blk, value_blk, erase_blk, write_blk = inputs
    block_len = query_blk.shape[1]
    head_size = query_blk.shape[2]
    log_gain = jnp.cumsum(logdec_blk, axis=1)
    log_before = log_gain - logdec_blk
    positions = jnp.arange(block_len)
    strict = positions[:, None] > positions[None, :]
    pair_decay = jnp.exp(
        jnp.where(
            strict[None, :, :, None], log_before[:, :, None, :] - log_gain[:, None, :, :], -jnp.inf
        )
    )

    def paired(left, right):
        return jnp.einsum("htc,htsc,hsc->hts", left, pair_decay, right, precision=HIGHEST)

    step_query = query_blk * jnp.exp(logdec_blk)
    identity_blk = jnp.eye(block_len, dtype=jnp.float32)
    erase_write = paired(erase_blk, write_blk)
    erase_key = paired(erase_blk, key_blk)
    read_write = (
        paired(step_query, write_blk)
        + identity_blk * jnp.sum(query_blk * write_blk, axis=-1)[:, :, None]
    )
    read_key = (
        paired(step_query, key_blk)
        + identity_blk * jnp.sum(query_blk * key_blk, axis=-1)[:, :, None]
    )
    inverse = identity_blk + erase_write
    power = erase_write
    for level in range(block_len.bit_length() - 2):
        power = exact_mul("hts,hsu->htu", power, power)
        inverse = inverse + exact_mul("hts,hsu->htu", inverse, power)
    erase_hat = erase_blk * jnp.exp(log_before)
    query_hat = query_blk * jnp.exp(log_gain)
    total_gain = log_gain[:, -1:, :]
    to_end = jnp.exp(total_gain - log_gain)
    write_end = write_blk * to_end
    key_end = key_blk * to_end
    pulled = exact_mul("hts,hsv->htv", inverse, exact_mul("hts,hsv->htv", erase_key, value_blk))
    local_out = exact_mul("hts,hsv->htv", read_write, pulled) + exact_mul(
        "hts,hsv->htv", read_key, value_blk
    )
    psi_block = exact_mul("hsv,hsc->hvc", pulled, write_end) + exact_mul(
        "hsv,hsc->hvc", value_blk, key_end
    )
    erase_solved = exact_mul("hts,hsc->htc", inverse, erase_hat)
    query_full = query_hat + exact_mul("hts,hsc->htc", read_write, erase_solved)
    identity_key = jnp.eye(head_size, dtype=jnp.float32)
    phi_block = jnp.exp(total_gain[:, 0, :])[:, :, None] * identity_key + exact_mul(
        "hsc,hsd->hcd", erase_solved, write_end
    )
    local_out = local_out + exact_mul("htc,hvc->htv", query_full, psi_sofar)
    carried_query = exact_mul("htc,hdc->htd", query_full, phi_sofar)
    phi_next = exact_mul("hcd,hde->hce", phi_sofar, phi_block)
    psi_next = exact_mul("hvd,hde->hve", psi_sofar, phi_block) + psi_block
    return ((phi_next, psi_next), (local_out, carried_query))


def body(
    tokens,
    input_norm_gain,
    query_matrix,
    key_matrix,
    value_matrix,
    convolution_value_matrix,
    convolution_gate_matrix,
    decay_offset_channel,
    decay_first_matrix,
    decay_second_matrix,
    learning_rate_offset,
    learning_rate_first_matrix,
    learning_rate_second_matrix,
    forgetting_rate_factor,
    state_retention_share,
    per_head_norm_gain,
    convolution_filter_taps,
    convolution_channel_gain,
    attention_output_matrix,
    convolution_output_matrix,
):
    tok_rows = tokens.shape[0]
    heads_dev = forgetting_rate_factor.shape[1]
    head_size = query_matrix.shape[1] // heads_dev
    widened = tokens.astype(jnp.float32)
    normed = (
        widened
        * lax.rsqrt(jnp.mean(widened * widened, axis=-1, keepdims=True) + RMS_EPSILON)
        * input_norm_gain
    ).astype(jnp.bfloat16)
    pieces = (
        lax.all_gather(query_matrix, "sp", axis=0, tiled=True),
        lax.all_gather(key_matrix, "sp", axis=0, tiled=True),
        lax.all_gather(value_matrix, "sp", axis=0, tiled=True),
        lax.all_gather(convolution_value_matrix, "sp", axis=0, tiled=True),
        lax.all_gather(convolution_gate_matrix, "sp", axis=0, tiled=True),
    )
    query_proj, key_proj, value_proj, conv_value, conv_gate = tuple(
        (jnp.dot(normed, piece, preferred_element_type=jnp.float32) for piece in pieces)
    )
    decay_mid = jnp.tanh(
        jnp.dot(normed, decay_first_matrix, preferred_element_type=jnp.float32)
    ).astype(jnp.bfloat16)
    rate_mid = jnp.dot(
        normed, learning_rate_first_matrix, preferred_element_type=jnp.float32
    ).astype(jnp.bfloat16)
    logarithm_learning_rate = (
        -jax.nn.softplus(
            -(
                decay_offset_channel
                + jnp.dot(decay_mid, decay_second_matrix, preferred_element_type=jnp.float32)
            )
        )
        - 0.5
    )
    learn_rate = jax.nn.sigmoid(
        learning_rate_offset
        + jnp.dot(rate_mid, learning_rate_second_matrix, preferred_element_type=jnp.float32)
    )
    reshaped_tensor = (tok_rows, heads_dev, head_size)
    log_decay = (
        -jnp.exp(logarithm_learning_rate).reshape(reshaped_tensor)
        * forgetting_rate_factor[:, :, None]
        + jnp.log(state_retention_share)[:, :, None]
    )
    key_heads = key_proj.reshape(reshaped_tensor)
    unit_key = key_heads * lax.rsqrt(
        jnp.sum(key_heads * key_heads, axis=-1, keepdims=True) + UNIT_EPSILON
    )
    erase = -unit_key
    write = unit_key * learn_rate.reshape(reshaped_tensor)
    block_len = math.gcd(tok_rows, 128)
    block_count = tok_rows // block_len
    inputs = tuple(
        (
            split_blocks(item, block_count, block_len)
            for item in (
                query_proj.reshape(reshaped_tensor),
                log_decay,
                key_heads,
                value_proj.reshape(reshaped_tensor),
                erase,
                write,
            )
        )
    )
    identity_key = jnp.broadcast_to(
        jnp.eye(head_size, dtype=jnp.float32), (heads_dev, head_size, head_size)
    )
    device_pair, block_outs = lax.scan(
        block_update, (identity_key, jnp.zeros_like(identity_key)), inputs
    )
    local_out, carried_query = block_outs
    phi_device, psi_device = device_pair
    prefix = entering(
        (phi_device, psi_device), "sp", chain_pair, (identity_key, jnp.zeros_like(identity_key))
    )
    state_in = prefix[1]
    state_out = local_out + exact_mul("bhtd,hvd->bhtv", carried_query, state_in)
    state_rows = state_out.transpose(0, 2, 1, 3).reshape(reshaped_tensor)
    centred = state_rows - jnp.mean(state_rows, axis=-1, keepdims=True)
    normal_state = centred * lax.rsqrt(
        jnp.mean(centred * centred, axis=-1, keepdims=True) + GROUP_EPSILON
    )
    state_mixed = (
        (normal_state * per_head_norm_gain.reshape(heads_dev, head_size))
        .reshape(tok_rows, heads_dev * head_size)
        .astype(jnp.bfloat16)
    )
    gated = (conv_value * jax.nn.sigmoid(conv_gate)).astype(jnp.bfloat16)
    span = convolution_filter_taps.shape[0]
    rim = from_behind(gated[tok_rows - (span - 1) :], "sp", 1)
    padded = jnp.concatenate([rim, gated], axis=0)
    filtered = jnp.zeros(gated.shape, jnp.float32)
    for offset in range(span):
        filtered = filtered + convolution_filter_taps[offset] * padded[offset : offset + tok_rows]
    total_sum, total_square = lax.psum(
        (jnp.sum(filtered, axis=-1), jnp.sum(filtered * filtered, axis=-1)), "tp"
    )
    row_mean = total_sum / CONV_CH
    deviation = filtered - row_mean[:, None]
    variance = total_square / CONV_CH - row_mean * row_mean
    conv_mixed = jax.nn.silu(
        deviation * lax.rsqrt(variance + LAYER_EPSILON)[:, None] * convolution_channel_gain
    ).astype(jnp.bfloat16)
    contract_dims = (((1,), (1,)), ((), ()))
    pieces = lax.all_gather(
        (attention_output_matrix, convolution_output_matrix), "sp", axis=0, tiled=True
    )
    partial_out = lax.dot_general(
        state_mixed, pieces[0], contract_dims, preferred_element_type=jnp.float32
    ) + lax.dot_general(conv_mixed, pieces[1], contract_dims, preferred_element_type=jnp.float32)
    return lax.psum(partial_out.astype(jnp.bfloat16), "tp")


def solution(mesh):
    return jax.shard_map(
        body,
        mesh=mesh,
        in_specs=(
            P("sp", None),
            P(),
            P("sp", "tp"),
            P("sp", "tp"),
            P("sp", "tp"),
            P("sp", "tp"),
            P("sp", "tp"),
            P("tp"),
            P(),
            P(None, "tp"),
            P("tp"),
            P(),
            P(None, "tp"),
            P("sp", "tp"),
            P("sp", "tp"),
            P("tp"),
            P(None, "tp"),
            P("tp"),
            P("sp", "tp"),
            P("sp", "tp"),
        ),
        out_specs=P("sp", None),
        check_vma=False,
    )
```

profile of v0, /device:TPU:0, one launch (start us, length us, event | category | flops | bytes accessed | tf_op | source)
XLA Modules:
  0.0 1069.4 jit_solution(5047170836986482139)
XLA Ops:
  17.3 55.9 %all-gather.12.cloned.1.call-done = bf16[2048,512]{1,0:T(8,128)(2,1)} async-done(((bf16[128,512]{1,0:T(8,128)(2,1)}), bf16[2048,512]{1,0:T(8,128)(2,1)}) %all-gather.12.cloned.1.call-update) | async-done | bytes 2097168 | tf_op jit(solution)/shard_map/all_gather | solution.py:148
  77.1 58.1 %all-gather.14.cloned.1.call-done = bf16[2048,512]{1,0:T(8,128)(2,1)} async-done(((bf16[128,512]{1,0:T(8,128)(2,1)}), bf16[2048,512]{1,0:T(8,128)(2,1)}) %all-gather.14.cloned.1.call-update) | async-done | bytes 2097168 | tf_op jit(solution)/shard_map/all_gather | solution.py:149
  138.1 59.1 %all-gather.16.cloned.1.call-done = bf16[2048,512]{1,0:T(8,128)(2,1)} async-done(((bf16[128,512]{1,0:T(8,128)(2,1)}), bf16[2048,512]{1,0:T(8,128)(2,1)}) %all-gather.16.cloned.1.call-update) | async-done | bytes 2097168 | tf_op jit(solution)/shard_map/all_gather | solution.py:147
  204.2 387.9 %while.31 = (s32[]{:T(128)}, f32[8,64,64]{1,2,0:T(8,128)}, f32[8,64,64]{1,2,0:T(8,128)S(1)}, f32[2,8,128,64]{2,3,0,1:T(8,128)}, f32[2,8,128,64]{2,3,0,1:T(8,128)...) while((s32[]{:T(128)}, f32[8,64,64]{1,2,0:T(8,128)}, ...), condition=%wide.region_6.7_spmd.clone, body=%wide.region_2.6_spmd.clone.sunk | while | flops 3836598272 | bytes 58414024 | solution.py:205
  206.6 23.3 %fusion.369 = f32[8,128,64]{2,0,1:T(8,128)S(1)} fusion(f32[8,128,64]{2,0,1:T(8,128)S(1)} %copy.214), kind=kOutput, calls=%fused_computation.245.clone.1 | output fusion | flops 8323072 | bytes 524288 | tf_op jit(solution)/shard_map/while/body/eval_jaxpr/jit(cumsum)/reduce_window_sum | solution.py:59
  235.5 33.2 %fusion.370 = f32[8,128,1,128]{3,2,1,0:T(1,128)S(1)} fusion(f32[8,128,64,1]{2,3,1,0:T(1,128)} %copy.213, f32[8,128,64]{1,2,0:T(8,128)S(1)} %bitcast.376, f32[8,128,64]{1,2,0:T(8,128)S(1)} %copy.215, f32[8,128,64]{2,1,0:T(8,128)S(1)} %copy.216, pred[128,128]{1,0:T(8,128)(4,1)S(1)} %iota_compare_fusion.5), kind=kOutput, calls=%fused_computation.6.clone.1 | convolution fusion | flops 125829120 | bytes 1589248 | tf_op jit(solution)/shard_map/while/body/eval_jaxpr/htc,htsc,hsc->hts/dot_general | solution.py:70
  276.7 35.6 %fusion.381 = f32[8,128,1,128]{3,2,1,0:T(1,128)S(1)} fusion(f32[8,128,64,1]{2,3,1,0:T(1,128)S(1)} %copy-done.6, f32[8,128,64]{1,2,0:T(8,128)S(1)} %bitcast.390, f32[8,128,64]{1,2,0:T(8,128)S(1)} %copy.215, f32[8,128,64]{2,1,0:T(8,128)S(1)} %copy-done.4, pred[128,128]{1,0:T(8,128)(4,1)S(1)} %iota_compare_fusion.5), kind=kOutput, calls=%fused_computation.2.clone.1 | convolution fusion | flops 125829120 | bytes 1589248 | tf_op jit(solution)/shard_map/while/body/eval_jaxpr/htc,htsc,hsc->hts/dot_general | solution.py:70
  317.8 33.1 %fusion.386 = f32[8,128,1,128]{3,2,1,0:T(1,128)S(1)} fusion(f32[8,128,64,1]{2,3,1,0:T(1,128)} %copy.217, f32[8,128,64]{1,2,0:T(8,128)S(1)} %bitcast.378, f32[8,128,64]{1,2,0:T(8,128)S(1)} %copy.215, f32[8,128,64]{2,1,0:T(8,128)} %copy-done.3, pred[128,128]{1,0:T(8,128)(4,1)S(1)} %iota_compare_fusion.5), kind=kOutput, calls=%fused_computation.4.clone.1 | convolution fusion | flops 125829120 | bytes 1589248 | tf_op jit(solution)/shard_map/while/body/eval_jaxpr/htc,htsc,hsc->hts/dot_general | solution.py:70
  352.0 31.7 %fusion.388 = f32[8,128,1,128]{3,2,1,0:T(1,128)S(1)} fusion(f32[8,128,64,1]{2,3,1,0:T(1,128)S(1)} %copy-done.7, f32[8,128,64]{1,2,0:T(8,128)S(1)} %bitcast.391, f32[8,128,64]{1,2,0:T(8,128)S(1)} %copy.215, f32[8,128,64]{2,1,0:T(8,128)S(1)} %copy-done.5, pred[128,128]{1,0:T(8,128)(4,1)S(1)} %iota_compare_fusion.5), kind=kOutput, calls=%fused_computation.clone.2 | convolution fusion | flops 125829120 | bytes 1589248 | tf_op jit(solution)/shard_map/while/body/eval_jaxpr/htc,htsc,hsc->hts/dot_general | solution.py:70
  397.4 23.3 %fusion.369 = f32[8,128,64]{2,0,1:T(8,128)S(1)} fusion(f32[8,128,64]{2,0,1:T(8,128)S(1)} %copy.214), kind=kOutput, calls=%fused_computation.245.clone.1 | output fusion | flops 8323072 | bytes 524288 | tf_op jit(solution)/shard_map/while/body/eval_jaxpr/jit(cumsum)/reduce_window_sum | solution.py:59
  426.4 33.0 %fusion.370 = f32[8,128,1,128]{3,2,1,0:T(1,128)S(1)} fusion(f32[8,128,64,1]{2,3,1,0:T(1,128)} %copy.213, f32[8,128,64]{1,2,0:T(8,128)S(1)} %bitcast.376, f32[8,128,64]{1,2,0:T(8,128)S(1)} %copy.215, f32[8,128,64]{2,1,0:T(8,128)S(1)} %copy.216, pred[128,128]{1,0:T(8,128)(4,1)S(1)} %iota_compare_fusion.5), kind=kOutput, calls=%fused_computation.6.clone.1 | convolution fusion | flops 125829120 | bytes 1589248 | tf_op jit(solution)/shard_map/while/body/eval_jaxpr/htc,htsc,hsc->hts/dot_general | solution.py:70
  467.4 35.6 %fusion.381 = f32[8,128,1,128]{3,2,1,0:T(1,128)S(1)} fusion(f32[8,128,64,1]{2,3,1,0:T(1,128)S(1)} %copy-done.6, f32[8,128,64]{1,2,0:T(8,128)S(1)} %bitcast.390, f32[8,128,64]{1,2,0:T(8,128)S(1)} %copy.215, f32[8,128,64]{2,1,0:T(8,128)S(1)} %copy-done.4, pred[128,128]{1,0:T(8,128)(4,1)S(1)} %iota_compare_fusion.5), kind=kOutput, calls=%fused_computation.2.clone.1 | convolution fusion | flops 125829120 | bytes 1589248 | tf_op jit(solution)/shard_map/while/body/eval_jaxpr/htc,htsc,hsc->hts/dot_general | solution.py:70
  508.5 33.1 %fusion.386 = f32[8,128,1,128]{3,2,1,0:T(1,128)S(1)} fusion(f32[8,128,64,1]{2,3,1,0:T(1,128)} %copy.217, f32[8,128,64]{1,2,0:T(8,128)S(1)} %bitcast.378, f32[8,128,64]{1,2,0:T(8,128)S(1)} %copy.215, f32[8,128,64]{2,1,0:T(8,128)} %copy-done.3, pred[128,128]{1,0:T(8,128)(4,1)S(1)} %iota_compare_fusion.5), kind=kOutput, calls=%fused_computation.4.clone.1 | convolution fusion | flops 125829120 | bytes 1589248 | tf_op jit(solution)/shard_map/while/body/eval_jaxpr/htc,htsc,hsc->hts/dot_general | solution.py:70
  542.7 31.7 %fusion.388 = f32[8,128,1,128]{3,2,1,0:T(1,128)S(1)} fusion(f32[8,128,64,1]{2,3,1,0:T(1,128)S(1)} %copy-done.7, f32[8,128,64]{1,2,0:T(8,128)S(1)} %bitcast.391, f32[8,128,64]{1,2,0:T(8,128)S(1)} %copy.215, f32[8,128,64]{2,1,0:T(8,128)S(1)} %copy-done.5, pred[128,128]{1,0:T(8,128)(4,1)S(1)} %iota_compare_fusion.5), kind=kOutput, calls=%fused_computation.clone.2 | convolution fusion | flops 125829120 | bytes 1589248 | tf_op jit(solution)/shard_map/while/body/eval_jaxpr/htc,htsc,hsc->hts/dot_general | solution.py:70
  597.9 70.6 %all-gather.26.cloned.1.call-done = f32[128,64,64]{2,1,0:T(8,128)} async-done(((f32[8,64,64]{2,1,0:T(8,128)}), f32[128,64,64]{2,1,0:T(8,128)}) %all-gather.26.cloned.1.call-update) | async-done | bytes 2097168 | tf_op jit(solution)/shard_map/all_gather | solution.py:20
  668.5 76.8 %all-gather.28.cloned.1.call-done = f32[128,64,64]{2,1,0:T(8,128)} async-done(((f32[8,64,64]{2,1,0:T(8,128)}), f32[128,64,64]{2,1,0:T(8,128)}) %all-gather.28.cloned.1.call-update) | async-done | bytes 2097168 | tf_op jit(solution)/shard_map/all_gather | solution.py:20
  745.4 43.6 %while.32 = (s32[]{:T(128)}, f32[8,64,64]{1,2,0:T(8,128)S(1)}, s32[]{:T(128)}, f32[16,8,64,64]{3,2,1,0:T(8,128)}, f32[16,8,64,64]{3,2,1,0:T(8,128)}, /*index=5*/s32[]{:T(128)}, s32[]{:T(128)}) while((s32[]{:T(128)}, f32[8,64,64]{1,2,0:T(8,128)S(1)}, s32[]{:T(128)}, f32[16,8,64,64]{3,2,1,0:T(8,128)}, f32[16,8,64,64]{3,2,1,0:T(8,128)}, ...), condition=%wide.region_8.9_spmd.clone, body=%wide.region_7.8_spmd.clone.sunk | while | flops 25296900 | bytes 1968227 | solution.py:30
  789.0 33.2 %all-gather.22.cloned.1.call-done = bf16[2048,1024]{1,0:T(8,128)(2,1)} async-done(((bf16[128,1024]{1,0:T(8,128)(2,1)}), bf16[2048,1024]{1,0:T(8,128)(2,1)}) %all-gather.22.cloned.1.call-update) | async-done | bytes 4194320 | tf_op jit(solution)/shard_map/all_gather | solution.py:151
  822.2 4.5 fusion.88
  826.8 72.4 %all-gather.20.cloned.1.call-done = bf16[2048,1024]{1,0:T(8,128)(2,1)} async-done(((bf16[128,1024]{1,0:T(8,128)(2,1)}), bf16[2048,1024]{1,0:T(8,128)(2,1)}) %all-gather.20.cloned.1.call-update) | async-done | bytes 4194320 | tf_op jit(solution)/shard_map/all_gather | solution.py:150
  908.3 6.0 fusion.155
  916.7 59.5 %all-gather.24.cloned.1.call-done = bf16[2048,1024]{1,0:T(8,128)(2,1)} async-done(((bf16[128,1024]{1,0:T(8,128)(2,1)}), bf16[2048,1024]{1,0:T(8,128)(2,1)}) %all-gather.24.cloned.1.call-update) | async-done | bytes 4194320 | tf_op jit(solution)/shard_map/all_gather | solution.py:242
  980.2 57.8 %all-gather.18.cloned.1.call-done = bf16[2048,512]{1,0:T(8,128)(2,1)} async-done(((bf16[128,512]{1,0:T(8,128)(2,1)}), bf16[2048,512]{1,0:T(8,128)(2,1)}) %all-gather.18.cloned.1.call-update) | async-done | bytes 2097168 | tf_op jit(solution)/shard_map/all_gather | solution.py:242
  1041.4 18.4 %all-reduce.3.cloned.1.call-done = bf16[256,2048]{1,0:T(8,128)(2,1)} async-done(((bf16[256,2048]{1,0:T(8,128)(2,1)}), bf16[256,2048]{1,0:T(8,128)(2,1)}) %all-reduce.3.cloned.1.call-update) | async-done | bytes 1048592 | tf_op jit(solution)/shard_map/psum | solution.py:248
  (292 shorter events, 160.3 us)
Async XLA Ops:
  6.5 66.7 %all-gather.12.cloned.1.call-start = ((), (), s32[]{:S(2)}) async-start(), calls=%async_computation | async-start | bytes 2228224 | tf_op jit(solution)/shard_map/all_gather | solution.py:148
  7.3 128.0 %all-gather.14.cloned.1.call-start = ((), (), s32[]{:S(2)}) async-start(), calls=%async_computation.1 | async-start | bytes 2228224 | tf_op jit(solution)/shard_map/all_gather | solution.py:149
  8.0 189.2 %all-gather.16.cloned.1.call-start = ((), (), s32[]{:S(2)}) async-start(), calls=%async_computation.2 | async-start | bytes 2228224 | tf_op jit(solution)/shard_map/all_gather | solution.py:147
  8.7 659.8 %all-gather.26.cloned.1.call-start = ((), (), s32[]{:S(2)}) async-start(), calls=%async_computation.8 | async-start | bytes 4456448 | tf_op jit(solution)/shard_map/all_gather | solution.py:20
  10.3 186.9 %copy-start.21 = (f32[256]{0:T(256)}, f32[256]{0:T(256)S(1)}, u32[]{:S(2)}) copy-start(f32[256]{0:T(256)S(1)} %add_rsqrt_fusion.1) | copy-start | bytes 3076
  234.5 34.2 %copy-start.3 = (f32[8,128,64]{2,1,0:T(8,128)}, f32[8,128,64]{2,1,0:T(8,128)S(1)}, u32[]{:S(2)}) copy-start(f32[8,128,64]{2,1,0:T(8,128)S(1)} %copy.216) | copy-start | bytes 786436 | tf_op jit(solution)/shard_map/while
  317.8 34.3 %copy-start.5 = (f32[8,128,64]{2,1,0:T(8,128)S(1)}, f32[8,128,64]{2,1,0:T(8,128)}, u32[]{:S(2)}) copy-start(f32[8,128,64]{2,1,0:T(8,128)} %copy-done.3) | copy-start | bytes 786436 | tf_op jit(solution)/shard_map/while
  317.8 34.3 %copy-start.7 = (f32[8,128,64,1]{2,3,1,0:T(1,128)S(1)}, f32[8,128,64,1]{2,3,1,0:T(1,128)}, u32[]{:S(2)}) copy-start(f32[8,128,64,1]{2,3,1,0:T(1,128)} %copy.217) | copy-start | bytes 786436 | tf_op jit(solution)/shard_map/while
  425.3 34.0 %copy-start.3 = (f32[8,128,64]{2,1,0:T(8,128)}, f32[8,128,64]{2,1,0:T(8,128)S(1)}, u32[]{:S(2)}) copy-start(f32[8,128,64]{2,1,0:T(8,128)S(1)} %copy.216) | copy-start | bytes 786436 | tf_op jit(solution)/shard_map/while
  508.5 34.3 %copy-start.5 = (f32[8,128,64]{2,1,0:T(8,128)S(1)}, f32[8,128,64]{2,1,0:T(8,128)}, u32[]{:S(2)}) copy-start(f32[8,128,64]{2,1,0:T(8,128)} %copy-done.3) | copy-start | bytes 786436 | tf_op jit(solution)/shard_map/while
  508.5 34.3 %copy-start.7 = (f32[8,128,64,1]{2,3,1,0:T(1,128)S(1)}, f32[8,128,64,1]{2,3,1,0:T(1,128)}, u32[]{:S(2)}) copy-start(f32[8,128,64,1]{2,3,1,0:T(1,128)} %copy.217) | copy-start | bytes 786436 | tf_op jit(solution)/shard_map/while
  594.0 151.4 %all-gather.28.cloned.1.call-start = ((), (), s32[]{:S(2)}) async-start(), calls=%async_computation.9 | async-start | bytes 4456448 | tf_op jit(solution)/shard_map/all_gather | solution.py:20
  594.9 227.3 %all-gather.22.cloned.1.call-start = ((), (), s32[]{:S(2)}) async-start(), calls=%async_computation.5 | async-start | bytes 4456448 | tf_op jit(solution)/shard_map/all_gather | solution.py:151
  595.5 303.7 %all-gather.20.cloned.1.call-start = ((), (), s32[]{:S(2)}) async-start(), calls=%async_computation.4 | async-start | bytes 4456448 | tf_op jit(solution)/shard_map/all_gather | solution.py:150
  596.2 380.0 %all-gather.24.cloned.1.call-start = ((), (), s32[]{:S(2)}) async-start(), calls=%async_computation.6 | async-start | bytes 4456448 | tf_op jit(solution)/shard_map/all_gather | solution.py:242
  597.0 441.0 %all-gather.18.cloned.1.call-start = ((), (), s32[]{:S(2)}) async-start(), calls=%async_computation.3 | async-start | bytes 2228224 | tf_op jit(solution)/shard_map/all_gather | solution.py:242
  597.7 462.1 %all-reduce.3.cloned.1.call-start = ((), (), s32[]{:S(2)}) async-start(), calls=%async_computation.7 | async-start | bytes 2097152 | tf_op jit(solution)/shard_map/psum | solution.py:248
  745.4 76.9 %copy-start.12 = (bf16[256,2048]{1,0:T(8,128)(2,1)S(1)}, bf16[256,2048]{1,0:T(8,128)(2,1)}, u32[]{:S(2)}) copy-start(bf16[256,2048]{1,0:T(8,128)(2,1)} %param.24) | copy-start | bytes 3145732
  745.4 76.9 %copy-start.22 = (f32[256]{0:T(256)S(1)}, f32[256]{0:T(256)}, u32[]{:S(2)}) copy-start(f32[256]{0:T(256)} %copy-done.21) | copy-start | bytes 3076
  745.4 76.9 %copy-start.25 = (f32[2048]{0:T(1024)S(1)}, f32[2048]{0:T(1024)}, u32[]{:S(2)}) copy-start(f32[2048]{0:T(1024)} %param.25) | copy-start | bytes 24580
  826.8 79.6 %copy-start.13 = (f32[2,8,128,64]{2,3,0,1:T(8,128)S(1)}, f32[2,8,128,64]{2,3,0,1:T(8,128)}, u32[]{:S(2)}) copy-start(f32[2,8,128,64]{2,3,0,1:T(8,128)} %get-tuple-element.159) | copy-start | bytes 1572868
  826.8 79.6 %copy-start.16 = (f32[2,8,128,64]{2,3,0,1:T(8,128)S(1)}, f32[2,8,128,64]{2,3,0,1:T(8,128)}, u32[]{:S(2)}) copy-start(f32[2,8,128,64]{2,3,0,1:T(8,128)} %get-tuple-element.163) | copy-start | bytes 1572868
  903.0 5.2 collective-permute-start
  907.1 69.1 %copy-start.26 = (f32[1024]{0:T(1024)S(1)}, f32[1024]{0:T(1024)}, u32[]{:S(2)}) copy-start(f32[1024]{0:T(1024)} %param.41) | copy-start | bytes 12292
  (26 other events, 139.3 us)
Sparse Core Ops, SparseCore 0:
  10.1 63.0 all-gather.11
  76.0 59.1 all-gather.13
  138.0 59.1 all-gather.15
  594.1 74.3 all-gather.25
  671.1 74.1 all-gather.27
  748.0 74.1 all-gather.21
  825.0 74.1 all-gather.19
  902.0 74.1 all-gather.23
  979.0 58.9 all-gather.17
  1041.5 18.1 all-reduce.2
where the time goes:
time: 1080 us; the launch traced here: 1070 us
  waiting for transfers between devices  567 us (52%)
  matrix products  365 us (34%)
  other arithmetic  59.7 us (6%)
  local copies, waits for them, and re-layouts  48.4 us (4%)
  between operations  14.4 us (1%)
    dot_general x8, matrix products, paired(): jnp.einsum('htc,htsc,hsc->hts', left, pair_decay, right, precision=HIGHEST)  267 us
    all_gather x2, waiting for transfers between devices, entering(): everything = jax.tree.map(lambda part: lax.all_gather(part, axis), x)  147 us
    all_gather x2, waiting for transfers between devices, body(): lax.all_gather((attention_output_matrix, convolution_output_matrix), 'sp'...  117 us
    all_gather x1, waiting for transfers between devices, body(): lax.all_gather(convolution_value_matrix, 'sp', axis=0, tiled=True)  72.4 us
    dot_general x67, matrix products, exact_mul(): return jnp.einsum(form, left, right, precision=HIGHEST)  70.9 us
    all_gather x1, waiting for transfers between devices, body(): lax.all_gather(query_matrix, 'sp', axis=0, tiled=True)  59.1 us
    all_gather x1, waiting for transfers between devices, body(): lax.all_gather(value_matrix, 'sp', axis=0, tiled=True)  58.1 us
    all_gather x1, waiting for transfers between devices, body(): lax.all_gather(key_matrix, 'sp', axis=0, tiled=True)  55.9 us
  transfers between devices with their start and end apart: 11, of which 11 were waited for; matrix products, arithmetic and copies ran while one was open for 7% of the time, Pallas kernels for 0%

commit v1 on v0

v1 whole, which is shorter than its diff:
```python
import functools
import math

import jax
import jax.numpy as jnp
from jax import lax
from jax.experimental import pallas as pl
from jax.experimental.pallas import tpu as pltpu
from jax.sharding import PartitionSpec as P


HIGHEST = lax.Precision.HIGHEST
RMS_EPSILON = 1e-06
GROUP_EPSILON = 0.00064
LAYER_EPSILON = 1e-05
UNIT_EPSILON = 1e-06
EXP_HALF = math.exp(-0.5)


def split(x):
    top = x.astype(jnp.bfloat16)
    return top, (x - top.astype(jnp.float32)).astype(jnp.bfloat16)


def dot3(left, right, dims=((1,), (0,))):
    (lh, ll), (rh, rl) = split(left), split(right)

    def one(p, q):
        return lax.dot_general(p, q, (dims, ((), ())), preferred_element_type=jnp.float32)

    return one(lh, rh) + (one(lh, rl) + one(ll, rh))


def dot3t(left, right):
    return dot3(left, right, ((1,), (1,)))


def exact(left, right):
    return jnp.dot(left, right, precision=HIGHEST, preferred_element_type=jnp.float32)


def column(values, index):
    lanes = lax.broadcasted_iota(jnp.int32, values.shape, 1)
    return jnp.sum(jnp.where(lanes == index, values, 0.0), axis=1, keepdims=True)


def delta_kernel(
    head_size, chunk, block,
    query_ref, key_ref, value_ref, decay_ref, rate_ref, factor_ref, share_ref,
    local_ref, carried_ref, pair_ref,
):
    rows, width = query_ref.shape
    pair = pl.program_id(0)
    per = width // head_size
    lane = lax.broadcasted_iota(jnp.int32, (1, width), 1)
    lane_head = lane // head_size
    row_w = lax.broadcasted_iota(jnp.int32, (width, width), 0)
    col_w = lax.broadcasted_iota(jnp.int32, (width, width), 1)
    same_head = (row_w // head_size) == (col_w // head_size)
    ones_head = jnp.where(same_head, 1.0, 0.0)
    row_b = lax.broadcasted_iota(jnp.int32, (block, block), 0)
    col_b = lax.broadcasted_iota(jnp.int32, (block, block), 1)
    same_chunk = (row_b // chunk) == (col_b // chunk)
    strict = same_chunk & (row_b > col_b)
    incl = same_chunk & (row_b >= col_b)
    sums = jnp.concatenate([jnp.where(incl, 1.0, 0.0), jnp.where(same_chunk, 1.0, 0.0)], axis=0)
    eye_b = jnp.where(row_b == col_b, 1.0, 0.0)

    factor, share = factor_ref[...], jnp.log(share_ref[...])
    factor_w = jnp.zeros((rows, width), jnp.float32)
    share_w = jnp.zeros((rows, width), jnp.float32)
    for h in range(per):
        factor_w = jnp.where(lane_head == h, column(factor, pair * per + h), factor_w)
        share_w = jnp.where(lane_head == h, column(share, pair * per + h), share_w)
    logdec = share_w - (EXP_HALF * jax.nn.sigmoid(decay_ref[...])) * factor_w
    learn = jax.nn.sigmoid(rate_ref[...])
    key = key_ref[...]
    unit = key * lax.rsqrt(exact(key * key, ones_head) + UNIT_EPSILON)

    blocks = []
    for start in range(0, rows, block):
        cut = slice(start, start + block)
        q, k, v, ld = query_ref[cut], key[cut], value_ref[cut], logdec[cut]
        er, wr = -unit[cut], unit[cut] * learn[cut]
        both = exact(sums, ld)
        gain, total = both[:block], both[block:]
        mid = 0.5 * total
        up, down, bup = jnp.exp(gain - mid), jnp.exp(mid - gain), jnp.exp(gain - ld - mid)
        ehat, qhat, what, khat = er * bup, q * up, wr * down, k * down
        right = jnp.concatenate([what, khat], axis=0)
        eh_full, q_full = er * jnp.exp(gain - ld), q * jnp.exp(gain)
        to_end = jnp.exp(total - gain)
        pulled = solved = local = query = None
        heads = []
        for h in range(per):
            left = jnp.where(lane_head == h, jnp.concatenate([ehat, qhat], axis=0), 0.0)
            grid = dot3t(left, right)
            ew = jnp.where(strict, grid[:block, :block], 0.0)
            ek = jnp.where(strict, grid[:block, block:], 0.0)
            rw = jnp.where(incl, grid[block:, :block], 0.0)
            rk = jnp.where(incl, grid[block:, block:], 0.0)
            size = 2
            off = (row_b // size == col_b // size) & (row_b > col_b)
            inv = eye_b + jnp.where(off, ew, 0.0)
            while size < chunk:
                off = (row_b // (2 * size) == col_b // (2 * size)) & (row_b // size > col_b // size)
                inv = inv + dot3(dot3(inv, jnp.where(off, ew, 0.0)), inv)
                size *= 2
            seen = dot3(jnp.concatenate([ek, rk], axis=0), v)
            both = dot3(inv, jnp.concatenate([seen[:block], eh_full], axis=1))
            read = dot3(rw, both)
            heads.append((both[:, :width], both[:, width:], read[:, :width] + seen[block:], read[:, width:]))
        merged = list(heads[0])
        for h in range(1, per):
            merged = [jnp.where(lane_head == h, new, old) for new, old in zip(heads[h], merged)]
        pulled, solved, local, query = merged
        blocks.append((pulled, solved, local, q_full + query, v, wr * to_end, k * to_end, jnp.exp(total)))

    state = jnp.concatenate([jnp.where(row_w == col_w, 1.0, 0.0), jnp.zeros((width, width), jnp.float32)], axis=0)
    across = ((0,), (0,))
    for number, (pulled, solved, local, query, v, wend, kend, gain) in enumerate(blocks):
        for first in range(0, block, chunk):
            cut = slice(first, first + chunk)
            place = slice(number * block + first, number * block + first + chunk)
            got = dot3t(query[cut], state)
            carried_ref[place] = got[:, :width]
            local_ref[place] = local[cut] + got[:, width:]
            step = jnp.where(same_head, dot3(solved[cut], wend[cut], across), 0.0)
            added = dot3(
                jnp.concatenate([pulled[cut], v[cut]], axis=0),
                jnp.concatenate([wend[cut], kend[cut]], axis=0),
                across,
            )
            added = jnp.where(same_head, added, 0.0)
            moved = state * gain[first : first + 1] + dot3(state, step)
            state = jnp.concatenate([moved[:width], moved[width:] + added], axis=0)
    pair_ref[0] = state


def finish_kernel(head_size, local_ref, carried_ref, state_ref, gain_ref, out_ref):
    width = local_ref.shape[1]
    row_w = lax.broadcasted_iota(jnp.int32, (width, width), 0)
    col_w = lax.broadcasted_iota(jnp.int32, (width, width), 1)
    same_head = (row_w // head_size) == (col_w // head_size)
    average = jnp.where(same_head, 1.0 / head_size, 0.0)
    y = local_ref[...] + dot3t(carried_ref[...], state_ref[0])
    centred = y - exact(y, average)
    variance = exact(centred * centred, average)
    out_ref[...] = (centred * lax.rsqrt(variance + GROUP_EPSILON) * gain_ref[...]).astype(jnp.bfloat16)


def from_behind(value, axis, steps):
    count = lax.axis_size(axis)
    initial, last = (max(0, -steps), min(count, count - steps))
    return lax.ppermute(value, axis, [(source, source + steps) for source in range(initial, last)])


def head_blocks(pairs, head_size):
    width = pairs.shape[-1]
    return jnp.stack(
        [pairs[:, a : a + head_size, a : a + head_size] for a in range(0, width, head_size)], axis=1
    )


def delta_rule(query, key, value, decay_pre, rate_pre, factor, share, gain):
    rows, channels = query.shape
    heads = factor.shape[1]
    head_size = channels // heads
    per = math.gcd(heads, max(1, 128 // head_size))
    width, pairs = per * head_size, heads // per
    block = math.gcd(rows, 128)
    chunk = math.gcd(block, 16)
    wide = pl.BlockSpec((rows, width), lambda i: (0, i))
    whole = pl.BlockSpec((rows, heads), lambda i: (0, 0))
    local, carried, pair = pl.pallas_call(
        functools.partial(delta_kernel, head_size, chunk, block),
        grid=(pairs,),
        in_specs=[wide] * 5 + [whole] * 2,
        out_specs=[wide, wide, pl.BlockSpec((1, 2 * width, width), lambda i: (i, 0, 0))],
        out_shape=[
            jax.ShapeDtypeStruct((rows, channels), jnp.float32),
            jax.ShapeDtypeStruct((rows, channels), jnp.float32),
            jax.ShapeDtypeStruct((pairs, 2 * width, width), jnp.float32),
        ],
        cost_estimate=pl.CostEstimate(
            flops=pairs * rows * width * width * 60, bytes_accessed=rows * channels * 32, transcendentals=rows * channels * 10
        ),
        name="delta_chunks",
    )(query, key, value, decay_pre, rate_pre, factor, share)

    phi, psi = head_blocks(pair[:, :width], head_size), head_blocks(pair[:, width:], head_size)
    both = jnp.concatenate([phi, psi], axis=-2).reshape(heads, 2 * head_size, head_size)
    count, place = lax.axis_size("sp"), lax.axis_index("sp")
    steps = 1
    while steps < count - 1:
        earlier = from_behind(both, "sp", steps)
        new = exact_mul("hcd,hde->hce", earlier, both[:, :head_size])
        new = new + jnp.concatenate([jnp.zeros_like(both[:, :head_size]), both[:, head_size:]], axis=1)
        both = jnp.where(place >= steps, new, both)
        steps *= 2
    state = from_behind(both[:, head_size:], "sp", 1).reshape(pairs, per, head_size, head_size)
    same = jnp.eye(per, dtype=jnp.float32)
    state = (state[:, :, :, None, :] * same[None, :, None, :, None]).reshape(pairs, width, width)
    return pl.pallas_call(
        functools.partial(finish_kernel, head_size),
        grid=(pairs,),
        in_specs=[wide, wide, pl.BlockSpec((1, width, width), lambda i: (i, 0, 0)), pl.BlockSpec((1, width), lambda i: (0, i))],
        out_specs=wide,
        out_shape=jax.ShapeDtypeStruct((rows, channels), jnp.bfloat16),
        name="delta_finish",
    )(local, carried, state, gain[None])


def exact_mul(form, left, right):
    return jnp.einsum(form, left, right, precision=HIGHEST)


def body(
    tokens,
    input_norm_gain,
    query_matrix,
    key_matrix,
    value_matrix,
    convolution_value_matrix,
    convolution_gate_matrix,
    decay_offset_channel,
    decay_first_matrix,
    decay_second_matrix,
    learning_rate_offset,
    learning_rate_first_matrix,
    learning_rate_second_matrix,
    forgetting_rate_factor,
    state_retention_share,
    per_head_norm_gain,
    convolution_filter_taps,
    convolution_channel_gain,
    attention_output_matrix,
    convolution_output_matrix,
):
    tok_rows = tokens.shape[0]
    widened = tokens.astype(jnp.float32)
    normed = (
        widened
        * lax.rsqrt(jnp.mean(widened * widened, axis=-1, keepdims=True) + RMS_EPSILON)
        * input_norm_gain
    ).astype(jnp.bfloat16)
    pieces = (
        lax.all_gather(query_matrix, "sp", axis=0, tiled=True),
        lax.all_gather(key_matrix, "sp", axis=0, tiled=True),
        lax.all_gather(value_matrix, "sp", axis=0, tiled=True),
        lax.all_gather(convolution_value_matrix, "sp", axis=0, tiled=True),
        lax.all_gather(convolution_gate_matrix, "sp", axis=0, tiled=True),
    )
    query_proj, key_proj, value_proj, conv_value, conv_gate = tuple(
        (jnp.dot(normed, piece, preferred_element_type=jnp.float32) for piece in pieces)
    )
    decay_mid = jnp.tanh(
        jnp.dot(normed, decay_first_matrix, preferred_element_type=jnp.float32)
    ).astype(jnp.bfloat16)
    rate_mid = jnp.dot(
        normed, learning_rate_first_matrix, preferred_element_type=jnp.float32
    ).astype(jnp.bfloat16)
    decay_pre = decay_offset_channel + jnp.dot(
        decay_mid, decay_second_matrix, preferred_element_type=jnp.float32
    )
    rate_pre = learning_rate_offset + jnp.dot(
        rate_mid, learning_rate_second_matrix, preferred_element_type=jnp.float32
    )
    state_mixed = delta_rule(
        query_proj, key_proj, value_proj, decay_pre, rate_pre,
        forgetting_rate_factor, state_retention_share, per_head_norm_gain,
    )
    gated = (conv_value * jax.nn.sigmoid(conv_gate)).astype(jnp.bfloat16)
    span = convolution_filter_taps.shape[0]
    rim = from_behind(gated[tok_rows - (span - 1) :], "sp", 1)
    padded = jnp.concatenate([rim, gated], axis=0)
    filtered = jnp.zeros(gated.shape, jnp.float32)
    for offset in range(span):
        filtered = filtered + convolution_filter_taps[offset] * padded[offset : offset + tok_rows]
    total_sum, total_square = lax.psum(
        (jnp.sum(filtered, axis=-1), jnp.sum(filtered * filtered, axis=-1)), "tp"
    )
    conv_channels = filtered.shape[1] * lax.axis_size("tp")
    row_mean = total_sum / conv_channels
    deviation = filtered - row_mean[:, None]
    variance = total_square / conv_channels - row_mean * row_mean
    conv_mixed = jax.nn.silu(
        deviation * lax.rsqrt(variance + LAYER_EPSILON)[:, None] * convolution_channel_gain
    ).astype(jnp.bfloat16)
    contract_dims = (((1,), (1,)), ((), ()))
    pieces = lax.all_gather(
        (attention_output_matrix, convolution_output_matrix), "sp", axis=0, tiled=True
    )
    partial_out = lax.dot_general(
        state_mixed, pieces[0], contract_dims, preferred_element_type=jnp.float32
    ) + lax.dot_general(conv_mixed, pieces[1], contract_dims, preferred_element_type=jnp.float32)
    return lax.psum(partial_out.astype(jnp.bfloat16), "tp")


def solution(mesh):
    return jax.shard_map(
        body,
        mesh=mesh,
        in_specs=(
            P("sp", None),
            P(),
            P("sp", "tp"),
            P("sp", "tp"),
            P("sp", "tp"),
            P("sp", "tp"),
            P("sp", "tp"),
            P("tp"),
            P(),
            P(None, "tp"),
            P("tp"),
            P(),
            P(None, "tp"),
            P("sp", "tp"),
            P("sp", "tp"),
            P("tp"),
            P(None, "tp"),
            P("tp"),
            P("sp", "tp"),
            P("sp", "tp"),
        ),
        out_specs=P("sp", None),
        check_vma=False,
    )
```

time: 1080 us -> 537 us (0.50)
  matrix products: 365 us -> 29.5 us
  waiting for transfers between devices: 567 us -> 375 us
  Pallas kernels: 0 us -> 61.8 us
  other arithmetic: 59.7 us -> 7.26 us
  local copies, waits for them, and re-layouts: 48.4 us -> 8.16 us
  starting transfers between devices: 3.69 us -> 37.5 us
    dot_general x8 -> x0, matrix products: 267 us -> none  [paired(): jnp.einsum('htc,htsc,hsc->hts', left, pair_decay, right, precision=HIGHEST)]
    all_gather x2 -> x0, waiting for transfers between devices: 147 us -> none  [entering(): everything = jax.tree.map(lambda part: lax.all_gather(part, axis), x)]
    dot_general x67 -> x4, matrix products: 70.9 us -> 1.48 us  [exact_mul(): return jnp.einsum(form, left, right, precision=HIGHEST)]
    pallas_call x0 -> x2, Pallas kernels: none -> 61.8 us  [the longest x1 56.6 us: delta_rule(): pl.pallas_call(functools.partial(delta_kernel, head_size, chunk, block),...]
    another operation x4 -> x0, other arithmetic: 46.6 us -> none  [the longest x2 46.6 us: block_update(): log_gain = jnp.cumsum(logdec_blk, axis=1)]
    ppermute x1 -> x6, starting transfers between devices: 3.34 us -> 37 us  [from_behind(): lax.ppermute(value, axis, [(source, source + steps) for source in range(i...]
    all_gather x1, waiting for transfers between devices: 72.4 us -> 39.2 us  [body(): lax.all_gather(convolution_value_matrix, 'sp', axis=0, tiled=True)]
    all_gather x1, waiting for transfers between devices: 33.2 us -> 0.02 us  [body(): lax.all_gather(convolution_gate_matrix, 'sp', axis=0, tiled=True)]
  transfers between devices with their start and end apart: 11 -> 14, of which waited for: 11 -> 12; matrix products, arithmetic and copies ran while one was open for 7% -> 7% of each run, Pallas kernels for 0% -> 12%
where the time goes in v1:
time: 537 us; the launch traced here: 536 us
  waiting for transfers between devices  375 us (70%)
  Pallas kernels  61.8 us (12%)
  starting transfers between devices  37.5 us (7%)
  matrix products  29.5 us (5%)
  between operations  13.8 us (3%)
  local copies, waits for them, and re-layouts  8.16 us (2%)
  other arithmetic  7.26 us (1%)
    all_gather x2, waiting for transfers between devices, body(): lax.all_gather((attention_output_matrix, convolution_output_matrix), 'sp'...  113 us
    all_gather x1, waiting for transfers between devices, body(): lax.all_gather(query_matrix, 'sp', axis=0, tiled=True)  58.8 us
    all_gather x1, waiting for transfers between devices, body(): lax.all_gather(key_matrix, 'sp', axis=0, tiled=True)  58.8 us
    pallas_call x1, Pallas kernels, delta_rule(): pl.pallas_call(functools.partial(delta_kernel, head_size, chunk, block),...  56.6 us
    all_gather x1, waiting for transfers between devices, body(): lax.all_gather(value_matrix, 'sp', axis=0, tiled=True)  56.5 us
    all_gather x1, waiting for transfers between devices, body(): lax.all_gather(convolution_value_matrix, 'sp', axis=0, tiled=True)  39.2 us
    ppermute x6, starting transfers between devices, from_behind(): lax.ppermute(value, axis, [(source, source + steps) for source in range(i...  37 us
    ppermute x6, waiting for transfers between devices, from_behind(): lax.ppermute(value, axis, [(source, source + steps) for source in range(i...  27.1 us
  transfers between devices with their start and end apart: 14, of which 12 were waited for; matrix products, arithmetic and copies ran while one was open for 7% of the time, Pallas kernels for 12%

profile of v1, /device:TPU:0, one launch (start us, length us, event | category | flops | bytes accessed | tf_op | source)
XLA Modules:
  0.0 535.9 jit_solution(12811334811987102115)
XLA Ops:
  16.8 56.5 %all-gather.12.cloned.1.call-done = bf16[2048,512]{1,0:T(8,128)(2,1)} async-done(((bf16[128,512]{1,0:T(8,128)(2,1)}), bf16[2048,512]{1,0:T(8,128)(2,1)}) %all-gather.12.cloned.1.call-update) | async-done | bytes 2097168 | tf_op jit(solution)/shard_map/all_gather | solution.py:250
  76.4 58.8 %all-gather.10.cloned.1.call-done = bf16[2048,512]{1,0:T(8,128)(2,1)} async-done(((bf16[128,512]{1,0:T(8,128)(2,1)}), bf16[2048,512]{1,0:T(8,128)(2,1)}) %all-gather.10.cloned.1.call-update) | async-done | bytes 2097168 | tf_op jit(solution)/shard_map/all_gather | solution.py:249
  138.4 58.8 %all-gather.8.cloned.1.call-done = bf16[2048,512]{1,0:T(8,128)(2,1)} async-done(((bf16[128,512]{1,0:T(8,128)(2,1)}), bf16[2048,512]{1,0:T(8,128)(2,1)}) %all-gather.8.cloned.1.call-update) | async-done | bytes 2097168 | tf_op jit(solution)/shard_map/all_gather | solution.py:248
  200.4 56.6 %delta_chunks.1 = (f32[256,512]{1,0:T(8,128)}, f32[256,512]{1,0:T(8,128)}, f32[4,256,128]{2,1,0:T(8,128)}) custom-call(f32[256,512]{1,0:T(8,128)} %fusion.63.query_ref, f32[256,512]{1,0:T(8,128)} %fusion.61.key_ref, f32[256,512]{1,0:T(8,128)} %fusion.59.value_ref, f32[256,512]{1,0:T(8,128)} %convolution_add_fusion.2.decay_ref, ...), custom_call_target="tpu_custom_call" | custom-call | flops 1006632960 | bytes 4194304 | tf_op jit(solution)/shard_map/delta_chunks/pallas_call | solution.py:175
  258.5 3.2 collective-permute-start
  261.8 5.1 collective-permute-done
  267.3 5.4 %collective-permute-start.1 = (f32[8,128,64]{1,2,0:T(8,128)S(1)}, f32[8,128,64]{1,2,0:T(8,128)S(1)}, u32[]{:S(2)}, u32[]{:S(2)}) collective-permute-start(f32[8,128,64]{1,2,0:T(8,128)S(1)} %fusion.10), channel_id=1, source_target_pairs={{0,4},{2,6},{4,8},{6,10},{8,12},{10,14},{12,16},{14,18},{16,20},{1... | collective-permute-start | bytes 786440 | tf_op jit(solution)/shard_map/ppermute | solution.py:155
  272.9 4.3 collective-permute-done.1
  277.6 10.4 %collective-permute-start.2 = (f32[8,128,64]{1,2,0:T(8,128)S(1)}, f32[8,128,64]{1,2,0:T(8,128)S(1)}, u32[]{:S(2)}, u32[]{:S(2)}) collective-permute-start(f32[8,128,64]{1,2,0:T(8,128)S(1)} %fusion.9), channel_id=1, source_target_pairs={{0,8},{2,10},{4,12},{6,14},{8,16},{10,18},{12,20},{14,22},{16,24},... | collective-permute-start | bytes 786440 | tf_op jit(solution)/shard_map/ppermute | solution.py:155
  288.4 5.5 %collective-permute-done.2 = f32[8,128,64]{1,2,0:T(8,128)S(1)} collective-permute-done((f32[8,128,64]{1,2,0:T(8,128)S(1)}, f32[8,128,64]{1,2,0:T(8,128)S(1)}, u32[]{:S(2)}, u32[]{:S(2)}) %collective-permute-start.2) | collective-permute-done | bytes 262176 | tf_op jit(solution)/shard_map/ppermute | solution.py:155
  294.2 13.3 %collective-permute-start.3 = (f32[8,128,64]{1,2,0:T(8,128)S(1)}, f32[8,128,64]{1,2,0:T(8,128)S(1)}, u32[]{:S(2)}, u32[]{:S(2)}) collective-permute-start(f32[8,128,64]{1,2,0:T(8,128)S(1)} %fusion.8), channel_id=1, source_target_pairs={{0,16},{2,18},{4,20},{6,22},{8,24},{10,26},{12,28},{14,30},{1,17},... | collective-permute-start | bytes 786440 | tf_op jit(solution)/shard_map/ppermute | solution.py:155
  307.9 3.4 collective-permute-done.3
  313.2 8.9 %collective-permute-done.4 = f32[8,64,64]{1,2,0:T(8,128)S(1)} collective-permute-done((f32[8,64,64]{1,2,0:T(8,128)S(1)}, f32[8,64,64]{1,2,0:T(8,128)S(1)}, u32[]{:S(2)}, u32[]{:S(2)}) %collective-permute-start.4) | collective-permute-done | bytes 131104 | tf_op jit(solution)/shard_map/ppermute | solution.py:155
  322.7 4.5 fusion.6
  327.3 39.2 %all-gather.16.cloned.1.call-done = bf16[2048,1024]{1,0:T(8,128)(2,1)} async-done(((bf16[128,1024]{1,0:T(8,128)(2,1)}), bf16[2048,1024]{1,0:T(8,128)(2,1)}) %all-gather.16.cloned.1.call-update) | async-done | bytes 4194320 | tf_op jit(solution)/shard_map/all_gather | solution.py:251
  366.4 3.8 fusion.7
  370.3 3.4 collective-permute-start.5
  374.3 5.2 delta_finish.1
  379.6 6.1 %fusion.65 = (f32[256]{0:T(256)S(1)}, f32[256]{0:T(256)S(1)}, f32[256,1024]{1,0:T(8,128)}) fusion(bf16[256,1024]{1,0:T(8,128)(2,1)S(1)} %fusion.7, f32[1024]{0:T(1024)S(1)} %bitcast.91, bf16[30,1024]{1,0:T(8,128)(2,1)S(1)} %collective-permute-done.5, f32[1024]{0:T(1024)S(1)} %bitcast.92, f32[1024]{0:T(1024)S(1)} %bitcast.63, f32[1024]{0:T(1024)S(1)} %bitcast.64, ...), kind=kLoop, calls=%fused_computation.120 | loop fusion | flops 48496128 | bytes 1763328 | tf_op jit(solution)/shard_map/reduce_sum | solution.py:281
  388.1 55.2 %all-gather.20.cloned.1.call-done = bf16[2048,1024]{1,0:T(8,128)(2,1)} async-done(((bf16[128,1024]{1,0:T(8,128)(2,1)}), bf16[2048,1024]{1,0:T(8,128)(2,1)}) %all-gather.20.cloned.1.call-update) | async-done | bytes 4194320 | tf_op jit(solution)/shard_map/all_gather | solution.py:291
  443.2 4.0 fusion.12
  447.3 57.7 %all-gather.14.cloned.1.call-done = bf16[2048,512]{1,0:T(8,128)(2,1)} async-done(((bf16[128,512]{1,0:T(8,128)(2,1)}), bf16[2048,512]{1,0:T(8,128)(2,1)}) %all-gather.14.cloned.1.call-update) | async-done | bytes 2097168 | tf_op jit(solution)/shard_map/all_gather | solution.py:291
  505.0 3.3 fusion
  508.4 18.4 %all-reduce.7.cloned.1.call-done = bf16[256,2048]{1,0:T(8,128)(2,1)} async-done(((bf16[256,2048]{1,0:T(8,128)(2,1)}), bf16[256,2048]{1,0:T(8,128)(2,1)}) %all-reduce.7.cloned.1.call-update) | async-done | bytes 1048592 | tf_op jit(solution)/shard_map/psum | solution.py:297
  (75 shorter events, 31.1 us)
Async XLA Ops:
  6.5 7.3 %copy-start = (bf16[2048,128]{1,0:T(8,128)(2,1)S(1)}, bf16[2048,128]{1,0:T(8,128)(2,1)}, u32[]{:S(2)}) copy-start(bf16[2048,128]{1,0:T(8,128)(2,1)} %param.31) | copy-start | bytes 1572868
  6.5 7.0 %copy-start.1 = (bf16[256,2048]{1,0:T(8,128)(2,1)S(1)}, bf16[256,2048]{1,0:T(8,128)(2,1)}, u32[]{:S(2)}) copy-start(bf16[256,2048]{1,0:T(8,128)(2,1)} %param.20) | copy-start | bytes 3145732
  6.5 7.3 %copy-start.7 = (f32[2048]{0:T(1024)S(1)}, f32[2048]{0:T(1024)}, u32[]{:S(2)}) copy-start(f32[2048]{0:T(1024)} %param.21) | copy-start | bytes 24580
  6.5 7.3 %copy-start.9 = (f32[512]{0:T(512)S(1)}, f32[512]{0:T(512)}, u32[]{:S(2)}) copy-start(f32[512]{0:T(512)} %param.30) | copy-start | bytes 6148
  6.5 7.3 %copy-start.5 = (bf16[128,512]{1,0:T(8,128)(2,1)S(1)}, bf16[128,512]{1,0:T(8,128)(2,1)}, u32[]{:S(2)}) copy-start(bf16[128,512]{1,0:T(8,128)(2,1)} %param.32) | copy-start | bytes 393220
  6.5 66.7 %all-gather.12.cloned.1.call-start = ((), (), s32[]{:S(2)}) async-start(), calls=%async_computation.2 | async-start | bytes 2228224 | tf_op jit(solution)/shard_map/all_gather | solution.py:250
  7.3 128.0 %all-gather.10.cloned.1.call-start = ((), (), s32[]{:S(2)}) async-start(), calls=%async_computation.1 | async-start | bytes 2228224 | tf_op jit(solution)/shard_map/all_gather | solution.py:249
  8.0 189.2 %all-gather.8.cloned.1.call-start = ((), (), s32[]{:S(2)}) async-start(), calls=%async_computation | async-start | bytes 2228224 | tf_op jit(solution)/shard_map/all_gather | solution.py:248
  8.8 314.0 %all-gather.18.cloned.1.call-start = ((), (), s32[]{:S(2)}) async-start(), calls=%async_computation.5 | async-start | bytes 4456448 | tf_op jit(solution)/shard_map/all_gather | solution.py:252
  9.3 357.1 %all-gather.16.cloned.1.call-start = ((), (), s32[]{:S(2)}) async-start(), calls=%async_computation.4 | async-start | bytes 4456448 | tf_op jit(solution)/shard_map/all_gather | solution.py:251
  9.9 5.4 %copy-start.4 = (bf16[2048,128]{1,0:T(8,128)(2,1)S(1)}, bf16[2048,128]{1,0:T(8,128)(2,1)}, u32[]{:S(2)}) copy-start(bf16[2048,128]{1,0:T(8,128)(2,1)} %param.28) | copy-start | bytes 1572868
  9.9 5.4 %copy-start.6 = (bf16[128,512]{1,0:T(8,128)(2,1)S(1)}, bf16[128,512]{1,0:T(8,128)(2,1)}, u32[]{:S(2)}) copy-start(bf16[128,512]{1,0:T(8,128)(2,1)} %param.29) | copy-start | bytes 393220
  10.0 433.3 %all-gather.20.cloned.1.call-start = ((), (), s32[]{:S(2)}) async-start(), calls=%async_computation.6 | async-start | bytes 4456448 | tf_op jit(solution)/shard_map/all_gather | solution.py:291
  10.5 494.5 %all-gather.14.cloned.1.call-start = ((), (), s32[]{:S(2)}) async-start(), calls=%async_computation.3 | async-start | bytes 2228224 | tf_op jit(solution)/shard_map/all_gather | solution.py:291
  258.5 8.5 %collective-permute-start = (f32[8,128,64]{1,2,0:T(8,128)S(1)}, f32[8,128,64]{1,2,0:T(8,128)S(1)}, u32[]{:S(2)}, u32[]{:S(2)}) collective-permute-start(f32[8,128,64]{1,2,0:T(8,128)S(1)} %bitcast.58), channel_id=1, source_target_pairs={{0,2},{2,4},{4,6},{6,8},{8,10},{10,12},{12,14},{14,16},{16,18},{18... | collective-permute-start | bytes 786440 | tf_op jit(solution)/shard_map/ppermute | solution.py:155
  261.8 45.7 %copy-start.3 = (f32[31,1024]{1,0:T(8,128)S(1)}, f32[31,1024]{1,0:T(8,128)}, u32[]{:S(2)}) copy-start(f32[31,1024]{1,0:T(8,128)} %param.36) | copy-start | bytes 380932
  267.3 9.9 %collective-permute-start.1 = (f32[8,128,64]{1,2,0:T(8,128)S(1)}, f32[8,128,64]{1,2,0:T(8,128)S(1)}, u32[]{:S(2)}, u32[]{:S(2)}) collective-permute-start(f32[8,128,64]{1,2,0:T(8,128)S(1)} %fusion.10), channel_id=1, source_target_pairs={{0,4},{2,6},{4,8},{6,10},{8,12},{10,14},{12,16},{14,18},{16,20},{1... | collective-permute-start | bytes 786440 | tf_op jit(solution)/shard_map/ppermute | solution.py:155
  277.6 16.2 %collective-permute-start.2 = (f32[8,128,64]{1,2,0:T(8,128)S(1)}, f32[8,128,64]{1,2,0:T(8,128)S(1)}, u32[]{:S(2)}, u32[]{:S(2)}) collective-permute-start(f32[8,128,64]{1,2,0:T(8,128)S(1)} %fusion.9), channel_id=1, source_target_pairs={{0,8},{2,10},{4,12},{6,14},{8,16},{10,18},{12,20},{14,22},{16,24},... | collective-permute-start | bytes 786440 | tf_op jit(solution)/shard_map/ppermute | solution.py:155
  288.0 238.7 %all-reduce.7.cloned.1.call-start = ((), (), s32[]{:S(2)}) async-start(), calls=%async_computation.7 | async-start | bytes 2097152 | tf_op jit(solution)/shard_map/psum | solution.py:297
  294.2 17.2 %collective-permute-start.3 = (f32[8,128,64]{1,2,0:T(8,128)S(1)}, f32[8,128,64]{1,2,0:T(8,128)S(1)}, u32[]{:S(2)}, u32[]{:S(2)}) collective-permute-start(f32[8,128,64]{1,2,0:T(8,128)S(1)} %fusion.8), channel_id=1, source_target_pairs={{0,16},{2,18},{4,20},{6,22},{8,24},{10,26},{12,28},{14,30},{1,17},... | collective-permute-start | bytes 786440 | tf_op jit(solution)/shard_map/ppermute | solution.py:155
  311.9 10.2 %collective-permute-start.4 = (f32[8,64,64]{1,2,0:T(8,128)S(1)}, f32[8,64,64]{1,2,0:T(8,128)S(1)}, u32[]{:S(2)}, u32[]{:S(2)}) collective-permute-start(f32[8,64,64]{1,2,0:T(8,128)S(1)} %fusion.46), channel_id=1, source_target_pairs={{0,2},{2,4},{4,6},{6,8},{8,10},{10,12},{12,14},{14,16},{16,18},{18... | collective-permute-start | bytes 393224 | tf_op jit(solution)/shard_map/ppermute | solution.py:155
  370.2 73.0 %copy-start.8 = (f32[1024]{0:T(1024)S(1)}, f32[1024]{0:T(1024)}, u32[]{:S(2)}) copy-start(f32[1024]{0:T(1024)} %param.37) | copy-start | bytes 12292
  370.3 9.3 %collective-permute-start.5 = (bf16[30,1024]{1,0:T(8,128)(2,1)S(1)}, bf16[30,1024]{1,0:T(8,128)(2,1)S(1)}, u32[]{:S(2)}, u32[]{:S(2)}) collective-permute-start(bf16[30,1024]{1,0:T(8,128)(2,1)S(1)} %slice.316), channel_id=1, source_target_pairs={{0,2},{2,4},{4,6},{6,8},{8,10},{10,12},{12,14},{14,16},{16,18},{18... | collective-permute-start | bytes 184328 | tf_op jit(solution)/shard_map/ppermute | solution.py:155
  443.2 61.8 %copy-start.2 = (bf16[256,512]{1,0:T(8,128)(2,1)S(1)}, bf16[256,512]{1,0:T(8,128)(2,1)}, u32[]{:S(2)}) copy-start(bf16[256,512]{1,0:T(8,128)(2,1)} %delta_finish.1) | copy-start | bytes 786436
  (1 other events, 5.4 us)
Sparse Core Ops, SparseCore 0:
  10.1 63.0 all-gather.11
  76.0 59.1 all-gather.9
  138.0 59.1 all-gather.7
  199.9 74.6 all-gather.17
  277.2 89.2 all-gather.15
  369.1 74.1 all-gather.19
  446.0 58.9 all-gather.13
  508.5 18.1 all-reduce.6

commit v2 on v1

--- a/solution.py
+++ b/solution.py
@@ -9,6 +9,7 @@
 from jax.sharding import PartitionSpec as P
 
 
+MESH = pl.DeviceIdType.MESH
 HIGHEST = lax.Precision.HIGHEST
 RMS_EPSILON = 1e-06
 GROUP_EPSILON = 0.00064
@@ -215,6 +216,116 @@
     return jnp.einsum(form, left, right, precision=HIGHEST)
 
 
+def gather_kernel(axis, radices, number, *refs):
+    ins, outs = refs[:number], refs[number : 2 * number]
+    own_sem, far_send, far_recv, near_send, near_recv = refs[2 * number :]
+    outer, middle, inner = radices
+    me = lax.axis_index(axis)
+    x, y, z = me % inner, (me // inner) % middle, me // (inner * middle)
+
+    def index(z_at, y_at, x_at):
+        return (z_at * middle + y_at) * inner + x_at
+
+    far = [index((z + step) % outer, y, x) for step in range(1, outer)]
+    near = {}
+    if inner == 2:
+        near["x"] = index(z, y, 1 - x)
+    if middle == 2:
+        near["y"] = index(z, 1 - y, x)
+    barrier = pltpu.get_barrier_semaphore()
+    peers = far + list(near.values())
+    for peer in peers:
+        pl.semaphore_signal(barrier, inc=1, device_id={axis: peer}, device_id_type=MESH)
+    pl.semaphore_wait(barrier, len(peers))
+
+    def far_copy(w, step, to, z_from):
+        return pltpu.make_async_remote_copy(
+            src_ref=ins[w],
+            dst_ref=outs[w].at[z_from, y, x],
+            send_sem=far_send.at[w, step],
+            recv_sem=far_recv.at[w, step],
+            device_id={axis: to},
+            device_id_type=MESH,
+        )
+
+    own = [pltpu.make_async_copy(ins[w], outs[w].at[z, y, x], own_sem.at[w]) for w in range(number)]
+    for w in range(number):
+        own[w].start()
+        for step in range(outer - 1):
+            far_copy(w, step, far[step], z).start()
+
+    def region(w, order, stage, from_y, from_x):
+        if stage == 0:
+            return outs[w].at[:, from_y, from_x]
+        return outs[w].at[:, from_y] if order[0] == "x" else outs[w].at[:, :, from_x]
+
+    def near_copy(w, order, stage, from_y, from_x):
+        part = region(w, order, stage, from_y, from_x)
+        return pltpu.make_async_remote_copy(
+            src_ref=part,
+            dst_ref=part,
+            send_sem=near_send.at[w, stage],
+            recv_sem=near_recv.at[w, stage],
+            device_id={axis: near[order[stage]]},
+            device_id_type=MESH,
+        )
+
+    def theirs(w, order, stage):
+        from_y, from_x = (y, 1 - x) if order[stage] == "x" else (1 - y, x)
+        return near_copy(w, order, stage, from_y, from_x)
+
+    names = list(near)
+    orders = [names if w % 2 == 0 else names[::-1] for w in range(number)]
+
+    def advance(w, stage):
+        if stage == 0:
+            own[w].wait()
+            for step in range(outer - 1):
+                far_copy(w, step, far[step], (z + outer - step - 1) % outer).wait_recv()
+        else:
+            theirs(w, orders[w], stage - 1).wait_recv()
+        if stage < len(names):
+            near_copy(w, orders[w], stage, y, x).start()
+
+    last = len(names)
+    for tick in range(number + last):
+        for stage in range(last, -1, -1):
+            w = tick - stage
+            if 0 <= w < number:
+                advance(w, stage)
+    for w in range(number):
+        for step in range(outer - 1):
+            far_copy(w, step, far[step], z).wait_send()
+        for stage in range(last):
+            near_copy(w, orders[w], stage, y, x).wait_send()
+
+
+def gather_rows(arrays, axis):
+    count, number = lax.axis_size(axis), len(arrays)
+    inner = math.gcd(count, 2)
+    middle = math.gcd(count // inner, 2)
+    radices = (count // inner // middle, middle, inner)
+    outs = pl.pallas_call(
+        functools.partial(gather_kernel, axis, radices, number),
+        in_specs=[pl.BlockSpec(memory_space=pltpu.VMEM)] * number,
+        out_specs=[pl.BlockSpec(memory_space=pl.ANY)] * number,
+        out_shape=[jax.ShapeDtypeStruct(radices + item.shape, item.dtype) for item in arrays],
+        scratch_shapes=[
+            pltpu.SemaphoreType.DMA((number,)),
+            pltpu.SemaphoreType.DMA((number, max(1, radices[0] - 1))),
+            pltpu.SemaphoreType.DMA((number, max(1, radices[0] - 1))),
+            pltpu.SemaphoreType.DMA((number, 2)),
+            pltpu.SemaphoreType.DMA((number, 2)),
+        ],
+        compiler_params=pltpu.CompilerParams(collective_id=0, has_side_effects=True),
+        cost_estimate=pl.CostEstimate(
+            flops=10**9, bytes_accessed=sum(item.size for item in arrays) * 2 * count, transcendentals=0
+        ),
+        name="gather_rows",
+    )(*arrays)
+    return [out.reshape((-1,) + item.shape[1:]) for out, item in zip(outs, arrays)]
+
+
 def body(
     tokens,
     input_norm_gain,
@@ -244,14 +355,10 @@
         * lax.rsqrt(jnp.mean(widened * widened, axis=-1, keepdims=True) + RMS_EPSILON)
         * input_norm_gain
     ).astype(jnp.bfloat16)
-    pieces = (
-        lax.all_gather(query_matrix, "sp", axis=0, tiled=True),
-        lax.all_gather(key_matrix, "sp", axis=0, tiled=True),
-        lax.all_gather(value_matrix, "sp", axis=0, tiled=True),
-        lax.all_gather(convolution_value_matrix, "sp", axis=0, tiled=True),
-        lax.all_gather(convolution_gate_matrix, "sp", axis=0, tiled=True),
-    )
-    query_proj, key_proj, value_proj, conv_value, conv_gate = tuple(
+    pieces = gather_rows(
+        (query_matrix, key_matrix, convolution_value_matrix, value_matrix, convolution_gate_matrix), "sp"
+    )
+    query_proj, key_proj, conv_value, value_proj, conv_gate = tuple(
         (jnp.dot(normed, piece, preferred_element_type=jnp.float32) for piece in pieces)
     )
     decay_mid = jnp.tanh(
@@ -294,7 +401,11 @@
     partial_out = lax.dot_general(
         state_mixed, pieces[0], contract_dims, preferred_element_type=jnp.float32
     ) + lax.dot_general(conv_mixed, pieces[1], contract_dims, preferred_element_type=jnp.float32)
-    return lax.psum(partial_out.astype(jnp.bfloat16), "tp")
+    partial_out = partial_out.astype(jnp.bfloat16)
+    if lax.axis_size("tp") != 2:
+        return lax.psum(partial_out, "tp")
+    other = lax.ppermute(partial_out, "tp", [(0, 1), (1, 0)])
+    return (partial_out.astype(jnp.float32) + other.astype(jnp.float32)).astype(jnp.bfloat16)
 
 
 def solution(mesh):

time: 537 us -> 449 us (0.84)
  waiting for transfers between devices: 375 us -> 14.4 us
  Pallas kernels: 61.8 us -> 335 us
    pallas_call x0 -> x1, Pallas kernels: none -> 273 us  [gather_rows(): pl.pallas_call(functools.partial(gather_kernel, axis, radices, number), i...]
    all_gather x5 -> x0, waiting for transfers between devices: 213 us -> none  [the longest x1 58.8 us: body(): lax.all_gather(query_matrix, 'sp', axis=0, tiled=True)]
    all_gather x2, waiting for transfers between devices: 113 us -> 0.02 us  [body(): lax.all_gather((attention_output_matrix, convolution_output_matrix), 'sp'...]
    psum x1 -> x0, waiting for transfers between devices: 18.4 us -> none  [body(): return lax.psum(partial_out.astype(jnp.bfloat16), 'tp')]
    ppermute x6, waiting for transfers between devices: 27.1 us -> 11 us  [from_behind(): lax.ppermute(value, axis, [(source, source + steps) for source in range(i...]
    ppermute x6, starting transfers between devices: 37 us -> 42.4 us  [from_behind(): lax.ppermute(value, axis, [(source, source + steps) for source in range(i...]
  transfers between devices with their start and end apart: 14 -> 9, of which waited for: 12 -> 3; matrix products, arithmetic and copies ran while one was open for 7% -> 8% of each run, Pallas kernels for 12% -> 75%
where the time goes in v2:
time: 449 us; the launch traced here: 448 us
  Pallas kernels  335 us (75%)
  starting transfers between devices  42.5 us (9%)
  matrix products  25.5 us (6%)
  waiting for transfers between devices  14.4 us (3%)
  between operations  13.8 us (3%)
  other arithmetic  8.65 us (2%)
  local copies, waits for them, and re-layouts  5.91 us (1%)
    pallas_call x1, Pallas kernels, gather_rows(): pl.pallas_call(functools.partial(gather_kernel, axis, radices, number), i...  273 us
    pallas_call x1, Pallas kernels, delta_rule(): pl.pallas_call(functools.partial(delta_kernel, head_size, chunk, block),...  56.6 us
    ppermute x6, starting transfers between devices, from_behind(): lax.ppermute(value, axis, [(source, source + steps) for source in range(i...  42.4 us
    dot_general x5, matrix products, body(): jnp.dot(normed, piece, preferred_element_type=jnp.float32)  14.7 us
    ppermute x6, waiting for transfers between devices, from_behind(): lax.ppermute(value, axis, [(source, source + steps) for source in range(i...  11 us
  transfers between devices with their start and end apart: 9, of which 3 were waited for; matrix products, arithmetic and copies ran while one was open for 8% of the time, Pallas kernels for 75%

profile of v2, /device:TPU:0, one launch (start us, length us, event | category | flops | bytes accessed | tf_op | source)
XLA Modules:
  0.0 447.9 jit_solution(3905843401438088539)
XLA Ops:
  7.3 1.5 copy.26.factor_ref
  8.8 1.5 copy.27.share_ref
  10.3 272.9 %gather_rows.1 = (bf16[4,2,2,128,512]{4,3,2,1,0:T(8,128)(2,1)}, bf16[4,2,2,128,512]{4,3,2,1,0:T(8,128)(2,1)}, bf16[4,2,2,128,1024]{4,3,2,1,0:T(8,128)(2,1)}, bf1...) custom-call(bf16[128,512]{1,0:T(8,128)(2,1)} %refs_0_.1, bf16[128,512]{1,0:T(8,128)(2,1)} %refs_1_.1, ...), custom_call_target="tpu_custom_call" | custom-call | flops 1000000000 | bytes 14680064 | tf_op jit(solution)/shard_map/gather_rows/pallas_call | solution.py:308
  285.0 1.5 convolution_add_fusion.2.decay_ref
  286.4 3.3 fusion.59.value_ref
  289.7 1.5 fusion.61.key_ref
  291.3 1.5 fusion.63.query_ref
  292.9 56.6 %delta_chunks.1 = (f32[256,512]{1,0:T(8,128)}, f32[256,512]{1,0:T(8,128)}, f32[4,256,128]{2,1,0:T(8,128)}) custom-call(f32[256,512]{1,0:T(8,128)} %fusion.63.query_ref, f32[256,512]{1,0:T(8,128)} %fusion.61.key_ref, f32[256,512]{1,0:T(8,128)} %fusion.59.value_ref, f32[256,512]{1,0:T(8,128)} %convolution_add_fusion.2.decay_ref, ...), custom_call_target="tpu_custom_call" | custom-call | flops 1006632960 | bytes 4194304 | tf_op jit(solution)/shard_map/delta_chunks/pallas_call | solution.py:176
  350.9 4.1 collective-permute-start
  355.0 4.5 %fusion.6 = f32[256,1024]{1,0:T(8,128)} fusion(bf16[2048,1024]{1,0:T(8,128)(2,1)} %bitcast.100, bf16[256,2048]{1,0:T(8,128)(2,1)S(1)} %copy-done.1, f32[2048]{0:T(1024)S(1)} %copy-done.7, f32[256]{0:T(256)S(1)} %add_rsqrt_fusion.1), kind=kOutput, calls=%fused_computation.41 | convolution fusion | flops 1076625408 | bytes 6300672 | tf_op jit(solution)/shard_map/dot_general | solution.py:362
  360.1 2.8 collective-permute-start.1
  362.9 3.8 fusion.7
  366.8 9.5 %collective-permute-start.5 = (bf16[30,1024]{1,0:T(8,128)(2,1)S(1)}, bf16[30,1024]{1,0:T(8,128)(2,1)S(1)}, u32[]{:S(2)}, u32[]{:S(2)}) collective-permute-start(bf16[30,1024]{1,0:T(8,128)(2,1)S(1)} %slice.316), channel_id=1, source_target_pairs={{0,2},{2,4},{4,6},{6,8},{8,10},{10,12},{12,14},{14,16},{16,18},{18... | collective-permute-start | bytes 184328 | tf_op jit(solution)/shard_map/ppermute | solution.py:156
  376.9 7.4 %collective-permute-start.2 = (f32[8,128,64]{1,2,0:T(8,128)S(1)}, f32[8,128,64]{1,2,0:T(8,128)S(1)}, u32[]{:S(2)}, u32[]{:S(2)}) collective-permute-start(f32[8,128,64]{1,2,0:T(8,128)S(1)} %fusion.9), channel_id=1, source_target_pairs={{0,8},{2,10},{4,12},{6,14},{8,16},{10,18},{12,20},{14,22},{16,24},... | collective-permute-start | bytes 786440 | tf_op jit(solution)/shard_map/ppermute | solution.py:156
  384.7 4.5 %collective-permute-done.2 = f32[8,128,64]{1,2,0:T(8,128)S(1)} collective-permute-done((f32[8,128,64]{1,2,0:T(8,128)S(1)}, f32[8,128,64]{1,2,0:T(8,128)S(1)}, u32[]{:S(2)}, u32[]{:S(2)}) %collective-permute-start.2) | collective-permute-done | bytes 262176 | tf_op jit(solution)/shard_map/ppermute | solution.py:156
  389.6 3.4 collective-permute-start.3
  393.0 6.1 %fusion.65 = (f32[256]{0:T(256)S(1)}, f32[256]{0:T(256)S(1)}, f32[256,1024]{1,0:T(8,128)}) fusion(bf16[256,1024]{1,0:T(8,128)(2,1)S(1)} %fusion.7, f32[1024]{0:T(1024)S(1)} %bitcast.77, bf16[30,1024]{1,0:T(8,128)(2,1)S(1)} %collective-permute-done.5, f32[1024]{0:T(1024)S(1)} %bitcast.78, f32[1024]{0:T(1024)S(1)} %bitcast.80, f32[1024]{0:T(1024)S(1)} %bitcast.81, ...), kind=kLoop, calls=%fused_computation.121 | loop fusion | flops 48496128 | bytes 1763328 | tf_op jit(solution)/shard_map/reduce_sum | solution.py:388
  399.1 2.4 all-reduce.4
  402.2 15.2 %collective-permute-start.4 = (f32[8,64,64]{1,2,0:T(8,128)S(1)}, f32[8,64,64]{1,2,0:T(8,128)S(1)}, u32[]{:S(2)}, u32[]{:S(2)}) collective-permute-start(f32[8,64,64]{1,2,0:T(8,128)S(1)} %fusion.46), channel_id=1, source_target_pairs={{0,2},{2,4},{4,6},{6,8},{8,10},{10,12},{12,14},{14,16},{16,18},{18... | collective-permute-start | bytes 393224 | tf_op jit(solution)/shard_map/ppermute | solution.py:156
  417.4 6.5 %collective-permute-done.4 = f32[8,64,64]{1,2,0:T(8,128)S(1)} collective-permute-done((f32[8,64,64]{1,2,0:T(8,128)S(1)}, f32[8,64,64]{1,2,0:T(8,128)S(1)}, u32[]{:S(2)}, u32[]{:S(2)}) %collective-permute-start.4) | collective-permute-done | bytes 131104 | tf_op jit(solution)/shard_map/ppermute | solution.py:156
  425.3 5.2 %delta_finish.1 = bf16[256,512]{1,0:T(8,128)(2,1)} custom-call(f32[256,512]{1,0:T(8,128)} %get-tuple-element.16.local_ref, f32[256,512]{1,0:T(8,128)} %get-tuple-element.17.carried_ref, f32[4,128,128]{2,1,0:T(8,128)} %broadcast_multiply_fusion.state_ref, f32[1,512]{1,0:T(1,128)} %bitcast.98), custom_call_target="tpu_custom_call" | custom-call | tf_op jit(solution)/shard_map/delta_finish/pallas_call | solution.py:205
  430.5 4.0 fusion.12
  434.6 2.4 fusion
  437.0 2.6 collective-permute-done.6
  (64 shorter events, 9.4 us)
Async XLA Ops:
  6.5 277.0 %copy-start = (bf16[2048,128]{1,0:T(8,128)(2,1)S(1)}, bf16[2048,128]{1,0:T(8,128)(2,1)}, u32[]{:S(2)}) copy-start(bf16[2048,128]{1,0:T(8,128)(2,1)} %param.31) | copy-start | bytes 1572868
  6.5 276.6 %copy-start.1 = (bf16[256,2048]{1,0:T(8,128)(2,1)S(1)}, bf16[256,2048]{1,0:T(8,128)(2,1)}, u32[]{:S(2)}) copy-start(bf16[256,2048]{1,0:T(8,128)(2,1)} %param.20) | copy-start | bytes 3145732
  6.5 423.9 %all-gather.5.cloned.1.call-start = ((), (), s32[]{:S(2)}) async-start(), calls=%async_computation.1 | async-start | bytes 4456448 | tf_op jit(solution)/shard_map/all_gather | solution.py:398
  7.3 427.3 %all-gather.3.cloned.1.call-start = ((), (), s32[]{:S(2)}) async-start(), calls=%async_computation | async-start | bytes 2228224 | tf_op jit(solution)/shard_map/all_gather | solution.py:398
  10.3 273.2 %copy-start.5 = (bf16[128,512]{1,0:T(8,128)(2,1)S(1)}, bf16[128,512]{1,0:T(8,128)(2,1)}, u32[]{:S(2)}) copy-start(bf16[128,512]{1,0:T(8,128)(2,1)} %param.32) | copy-start | bytes 393220
  10.3 273.2 %copy-start.7 = (f32[2048]{0:T(1024)S(1)}, f32[2048]{0:T(1024)}, u32[]{:S(2)}) copy-start(f32[2048]{0:T(1024)} %param.21) | copy-start | bytes 24580
  10.3 273.2 %copy-start.9 = (f32[512]{0:T(512)S(1)}, f32[512]{0:T(512)}, u32[]{:S(2)}) copy-start(f32[512]{0:T(512)} %param.30) | copy-start | bytes 6148
  283.2 1.8 copy-start.4
  283.2 1.8 copy-start.6
  283.2 1.8 copy-start.10
  286.4 3.3 copy-start.12
  289.7 1.6 copy-start.11
  350.9 8.8 %collective-permute-start = (f32[8,128,64]{1,2,0:T(8,128)S(1)}, f32[8,128,64]{1,2,0:T(8,128)S(1)}, u32[]{:S(2)}, u32[]{:S(2)}) collective-permute-start(f32[8,128,64]{1,2,0:T(8,128)S(1)} %bitcast.63), channel_id=1, source_target_pairs={{0,2},{2,4},{4,6},{6,8},{8,10},{10,12},{12,14},{14,16},{16,18},{18... | collective-permute-start | bytes 786440 | tf_op jit(solution)/shard_map/ppermute | solution.py:156
  360.1 16.4 %collective-permute-start.1 = (f32[8,128,64]{1,2,0:T(8,128)S(1)}, f32[8,128,64]{1,2,0:T(8,128)S(1)}, u32[]{:S(2)}, u32[]{:S(2)}) collective-permute-start(f32[8,128,64]{1,2,0:T(8,128)S(1)} %fusion.10), channel_id=1, source_target_pairs={{0,4},{2,6},{4,8},{6,10},{8,12},{10,14},{12,16},{14,18},{16,20},{1... | collective-permute-start | bytes 786440 | tf_op jit(solution)/shard_map/ppermute | solution.py:156
  362.9 13.3 %copy-start.3 = (f32[31,1024]{1,0:T(8,128)S(1)}, f32[31,1024]{1,0:T(8,128)}, u32[]{:S(2)}) copy-start(f32[31,1024]{1,0:T(8,128)} %param.36) | copy-start | bytes 380932
  366.8 26.2 %collective-permute-start.5 = (bf16[30,1024]{1,0:T(8,128)(2,1)S(1)}, bf16[30,1024]{1,0:T(8,128)(2,1)S(1)}, u32[]{:S(2)}, u32[]{:S(2)}) collective-permute-start(bf16[30,1024]{1,0:T(8,128)(2,1)S(1)} %slice.316), channel_id=1, source_target_pairs={{0,2},{2,4},{4,6},{6,8},{8,10},{10,12},{12,14},{14,16},{16,18},{18... | collective-permute-start | bytes 184328 | tf_op jit(solution)/shard_map/ppermute | solution.py:156
  376.9 12.4 %collective-permute-start.2 = (f32[8,128,64]{1,2,0:T(8,128)S(1)}, f32[8,128,64]{1,2,0:T(8,128)S(1)}, u32[]{:S(2)}, u32[]{:S(2)}) collective-permute-start(f32[8,128,64]{1,2,0:T(8,128)S(1)} %fusion.9), channel_id=1, source_target_pairs={{0,8},{2,10},{4,12},{6,14},{8,16},{10,18},{12,20},{14,22},{16,24},... | collective-permute-start | bytes 786440 | tf_op jit(solution)/shard_map/ppermute | solution.py:156
  389.6 12.0 %collective-permute-start.3 = (f32[8,128,64]{1,2,0:T(8,128)S(1)}, f32[8,128,64]{1,2,0:T(8,128)S(1)}, u32[]{:S(2)}, u32[]{:S(2)}) collective-permute-start(f32[8,128,64]{1,2,0:T(8,128)S(1)} %fusion.8), channel_id=1, source_target_pairs={{0,16},{2,18},{4,20},{6,22},{8,24},{10,26},{12,28},{14,30},{1,17},... | collective-permute-start | bytes 786440 | tf_op jit(solution)/shard_map/ppermute | solution.py:156
  402.2 21.7 %collective-permute-start.4 = (f32[8,64,64]{1,2,0:T(8,128)S(1)}, f32[8,64,64]{1,2,0:T(8,128)S(1)}, u32[]{:S(2)}, u32[]{:S(2)}) collective-permute-start(f32[8,64,64]{1,2,0:T(8,128)S(1)} %fusion.46), channel_id=1, source_target_pairs={{0,2},{2,4},{4,6},{6,8},{8,10},{10,12},{12,14},{14,16},{16,18},{18... | collective-permute-start | bytes 393224 | tf_op jit(solution)/shard_map/ppermute | solution.py:156
  423.9 6.6 %copy-start.8 = (f32[1024]{0:T(1024)S(1)}, f32[1024]{0:T(1024)}, u32[]{:S(2)}) copy-start(f32[1024]{0:T(1024)} %param.37) | copy-start | bytes 12292
  430.5 4.1 copy-start.2
  436.9 2.7 collective-permute-start.6
Sparse Core Ops, SparseCore 0:
  10.1 123.8 all-gather.4
  355.2 77.5 all-gather.2

commit v3 on v2

--- a/solution.py
+++ b/solution.py
@@ -355,10 +355,12 @@
         * lax.rsqrt(jnp.mean(widened * widened, axis=-1, keepdims=True) + RMS_EPSILON)
         * input_norm_gain
     ).astype(jnp.bfloat16)
-    pieces = gather_rows(
-        (query_matrix, key_matrix, convolution_value_matrix, value_matrix, convolution_gate_matrix), "sp"
-    )
-    query_proj, key_proj, conv_value, value_proj, conv_gate = tuple(
+    pieces = (
+        *gather_rows((query_matrix, key_matrix, value_matrix), "sp"),
+        lax.all_gather(convolution_value_matrix, "sp", axis=0, tiled=True),
+        lax.all_gather(convolution_gate_matrix, "sp", axis=0, tiled=True),
+    )
+    query_proj, key_proj, value_proj, conv_value, conv_gate = tuple(
         (jnp.dot(normed, piece, preferred_element_type=jnp.float32) for piece in pieces)
     )
     decay_mid = jnp.tanh(

time: 449 us -> 364 us (0.81)
  Pallas kernels: 335 us -> 185 us
  starting transfers between devices: 42.5 us -> 85.5 us
  waiting for transfers between devices: 14.4 us -> 36.3 us
    pallas_call x1, Pallas kernels: 273 us -> 123 us  [gather_rows(): pl.pallas_call(functools.partial(gather_kernel, axis, radices, number), i...]
    ppermute x6, starting transfers between devices: 42.4 us -> 85.3 us  [from_behind(): lax.ppermute(value, axis, [(source, source + steps) for source in range(i...]
    ppermute x6, waiting for transfers between devices: 11 us -> 22.7 us  [from_behind(): lax.ppermute(value, axis, [(source, source + steps) for source in range(i...]
    all_gather x2, waiting for transfers between devices: 0.02 us -> 8.85 us  [body(): lax.all_gather((attention_output_matrix, convolution_output_matrix), 'sp'...]
  transfers between devices with their start and end apart: 9 -> 11, of which waited for: 3 -> 7; matrix products, arithmetic and copies ran while one was open for 8% -> 10% of each run, Pallas kernels for 75% -> 51%
where the time goes in v3:
time: 364 us; the launch traced here: 363 us
  Pallas kernels  185 us (51%)
  starting transfers between devices  85.5 us (23%)
  waiting for transfers between devices  36.3 us (10%)
  matrix products  25.7 us (7%)
  between operations  13.5 us (4%)
  other arithmetic  8.63 us (2%)
  local copies, waits for them, and re-layouts  5.86 us (2%)
    pallas_call x1, Pallas kernels, gather_rows(): pl.pallas_call(functools.partial(gather_kernel, axis, radices, number), i...  123 us
    ppermute x6, starting transfers between devices, from_behind(): lax.ppermute(value, axis, [(source, source + steps) for source in range(i...  85.3 us
    pallas_call x1, Pallas kernels, delta_rule(): pl.pallas_call(functools.partial(delta_kernel, head_size, chunk, block),...  56.6 us
    ppermute x6, waiting for transfers between devices, from_behind(): lax.ppermute(value, axis, [(source, source + steps) for source in range(i...  22.7 us
    dot_general x5, matrix products, body(): jnp.dot(normed, piece, preferred_element_type=jnp.float32)  14.9 us
    all_gather x2, waiting for transfers between devices, body(): lax.all_gather((attention_output_matrix, convolution_output_matrix), 'sp'...  8.85 us
  transfers between devices with their start and end apart: 11, of which 7 were waited for; matrix products, arithmetic and copies ran while one was open for 10% of the time, Pallas kernels for 51%

profile of v3, /device:TPU:0, one launch (start us, length us, event | category | flops | bytes accessed | tf_op | source)
XLA Modules:
  0.0 363.1 jit_solution(15472160627627974939)
XLA Ops:
  11.7 123.4 %gather_rows.1 = (bf16[4,2,2,128,512]{4,3,2,1,0:T(8,128)(2,1)}, bf16[4,2,2,128,512]{4,3,2,1,0:T(8,128)(2,1)}, bf16[4,2,2,128,512]{4,3,2,1,0:T(8,128)(2,1)}) custom-call(bf16[128,512]{1,0:T(8,128)(2,1)} %refs_0_.1, bf16[128,512]{1,0:T(8,128)(2,1)} %refs_1_.1, bf16[128,512]{1,0:T(8,128)(2,1)} %refs_2_.1), custom_call_target="tpu_custom_call" | custom-call | flops 1000000000 | bytes 6291456 | tf_op jit(solution)/shard_map/gather_rows/pallas_call | solution.py:308
  138.5 3.3 fusion.59.value_ref
  141.8 1.6 fusion.61.key_ref
  145.0 56.6 %delta_chunks.1 = (f32[256,512]{1,0:T(8,128)}, f32[256,512]{1,0:T(8,128)}, f32[4,256,128]{2,1,0:T(8,128)}) custom-call(f32[256,512]{1,0:T(8,128)} %fusion.63.query_ref, f32[256,512]{1,0:T(8,128)} %fusion.61.key_ref, f32[256,512]{1,0:T(8,128)} %fusion.59.value_ref, f32[256,512]{1,0:T(8,128)} %convolution_add_fusion.2.decay_ref, ...), custom_call_target="tpu_custom_call" | custom-call | flops 1006632960 | bytes 4194304 | tf_op jit(solution)/shard_map/delta_chunks/pallas_call | solution.py:176
  203.0 10.7 %collective-permute-start = (f32[8,128,64]{1,2,0:T(8,128)S(1)}, f32[8,128,64]{1,2,0:T(8,128)S(1)}, u32[]{:S(2)}, u32[]{:S(2)}) collective-permute-start(f32[8,128,64]{1,2,0:T(8,128)S(1)} %bitcast.61), channel_id=1, source_target_pairs={{0,2},{2,4},{4,6},{6,8},{8,10},{10,12},{12,14},{14,16},{16,18},{18... | collective-permute-start | bytes 786440 | tf_op jit(solution)/shard_map/ppermute | solution.py:156
  213.9 3.7 %collective-permute-done = f32[8,128,64]{1,2,0:T(8,128)S(1)} collective-permute-done((f32[8,128,64]{1,2,0:T(8,128)S(1)}, f32[8,128,64]{1,2,0:T(8,128)S(1)}, u32[]{:S(2)}, u32[]{:S(2)}) %collective-permute-start) | collective-permute-done | bytes 262176 | tf_op jit(solution)/shard_map/ppermute | solution.py:156
  218.0 4.5 %collective-permute-start.1 = (f32[8,128,64]{1,2,0:T(8,128)S(1)}, f32[8,128,64]{1,2,0:T(8,128)S(1)}, u32[]{:S(2)}, u32[]{:S(2)}) collective-permute-start(f32[8,128,64]{1,2,0:T(8,128)S(1)} %fusion.10), channel_id=1, source_target_pairs={{0,4},{2,6},{4,8},{6,10},{8,12},{10,14},{12,16},{14,18},{16,20},{1... | collective-permute-start | bytes 786440 | tf_op jit(solution)/shard_map/ppermute | solution.py:156
  222.6 6.8 %collective-permute-done.1 = f32[8,128,64]{1,2,0:T(8,128)S(1)} collective-permute-done((f32[8,128,64]{1,2,0:T(8,128)S(1)}, f32[8,128,64]{1,2,0:T(8,128)S(1)}, u32[]{:S(2)}, u32[]{:S(2)}) %collective-permute-start.1) | collective-permute-done | bytes 262176 | tf_op jit(solution)/shard_map/ppermute | solution.py:156
  229.8 41.5 %collective-permute-start.2 = (f32[8,128,64]{1,2,0:T(8,128)S(1)}, f32[8,128,64]{1,2,0:T(8,128)S(1)}, u32[]{:S(2)}, u32[]{:S(2)}) collective-permute-start(f32[8,128,64]{1,2,0:T(8,128)S(1)} %fusion.9), channel_id=1, source_target_pairs={{0,8},{2,10},{4,12},{6,14},{8,16},{10,18},{12,20},{14,22},{16,24},... | collective-permute-start | bytes 786440 | tf_op jit(solution)/shard_map/ppermute | solution.py:156
  271.4 4.0 %collective-permute-done.2 = f32[8,128,64]{1,2,0:T(8,128)S(1)} collective-permute-done((f32[8,128,64]{1,2,0:T(8,128)S(1)}, f32[8,128,64]{1,2,0:T(8,128)S(1)}, u32[]{:S(2)}, u32[]{:S(2)}) %collective-permute-start.2) | collective-permute-done | bytes 262176 | tf_op jit(solution)/shard_map/ppermute | solution.py:156
  275.8 18.7 %collective-permute-start.3 = (f32[8,128,64]{1,2,0:T(8,128)S(1)}, f32[8,128,64]{1,2,0:T(8,128)S(1)}, u32[]{:S(2)}, u32[]{:S(2)}) collective-permute-start(f32[8,128,64]{1,2,0:T(8,128)S(1)} %fusion.8), channel_id=1, source_target_pairs={{0,16},{2,18},{4,20},{6,22},{8,24},{10,26},{12,28},{14,30},{1,17},... | collective-permute-start | bytes 786440 | tf_op jit(solution)/shard_map/ppermute | solution.py:156
  295.0 4.4 %collective-permute-done.3 = f32[8,128,64]{1,2,0:T(8,128)S(1)} collective-permute-done((f32[8,128,64]{1,2,0:T(8,128)S(1)}, f32[8,128,64]{1,2,0:T(8,128)S(1)}, u32[]{:S(2)}, u32[]{:S(2)}) %collective-permute-start.3) | collective-permute-done | bytes 262176 | tf_op jit(solution)/shard_map/ppermute | solution.py:156
  299.9 5.5 %collective-permute-start.4 = (f32[8,64,64]{1,2,0:T(8,128)S(1)}, f32[8,64,64]{1,2,0:T(8,128)S(1)}, u32[]{:S(2)}, u32[]{:S(2)}) collective-permute-start(f32[8,64,64]{1,2,0:T(8,128)S(1)} %fusion.46), channel_id=1, source_target_pairs={{0,2},{2,4},{4,6},{6,8},{8,10},{10,12},{12,14},{14,16},{16,18},{18... | collective-permute-start | bytes 393224 | tf_op jit(solution)/shard_map/ppermute | solution.py:156
  305.5 3.8 %collective-permute-done.4 = f32[8,64,64]{1,2,0:T(8,128)S(1)} collective-permute-done((f32[8,64,64]{1,2,0:T(8,128)S(1)}, f32[8,64,64]{1,2,0:T(8,128)S(1)}, u32[]{:S(2)}, u32[]{:S(2)}) %collective-permute-start.4) | collective-permute-done | bytes 131104 | tf_op jit(solution)/shard_map/ppermute | solution.py:156
  309.9 4.6 %fusion.6 = f32[256,1024]{1,0:T(8,128)} fusion(bf16[2048,1024]{1,0:T(8,128)(2,1)} %all-gather.9.cloned.1.call-done, bf16[256,2048]{1,0:T(8,128)(2,1)S(1)} %copy-done.1, f32[2048]{0:T(1024)S(1)} %copy-done.7, f32[256]{0:T(256)S(1)} %add_rsqrt_fusion.1), kind=kOutput, calls=%fused_computation.41 | convolution fusion | flops 1076625408 | bytes 6300672 | tf_op jit(solution)/shard_map/dot_general | solution.py:364
  314.5 3.8 %fusion.7 = bf16[256,1024]{1,0:T(8,128)(2,1)S(1)} fusion(f32[256,1024]{1,0:T(8,128)} %fusion.6, bf16[2048,1024]{1,0:T(8,128)(2,1)} %all-gather.7.cloned.1.call-done, bf16[256,2048]{1,0:T(8,128)(2,1)S(1)} %copy-done.1, f32[2048]{0:T(1024)S(1)} %copy-done.7, f32[256]{0:T(256)S(1)} %add_rsqrt_fusion.1), kind=kOutput, calls=%fused_computation.42 | convolution fusion | flops 1076363264 | bytes 6824960 | tf_op jit(solution)/shard_map/dot_general | solution.py:364
  318.4 4.4 %collective-permute-start.5 = (bf16[30,1024]{1,0:T(8,128)(2,1)S(1)}, bf16[30,1024]{1,0:T(8,128)(2,1)S(1)}, u32[]{:S(2)}, u32[]{:S(2)}) collective-permute-start(bf16[30,1024]{1,0:T(8,128)(2,1)S(1)} %slice.316), channel_id=1, source_target_pairs={{0,2},{2,4},{4,6},{6,8},{8,10},{10,12},{12,14},{14,16},{16,18},{18... | collective-permute-start | bytes 184328 | tf_op jit(solution)/shard_map/ppermute | solution.py:156
  323.5 5.2 %delta_finish.1 = bf16[256,512]{1,0:T(8,128)(2,1)} custom-call(f32[256,512]{1,0:T(8,128)} %get-tuple-element.14.local_ref, f32[256,512]{1,0:T(8,128)} %get-tuple-element.15.carried_ref, f32[4,128,128]{2,1,0:T(8,128)} %broadcast_multiply_fusion.state_ref, f32[1,512]{1,0:T(1,128)} %bitcast.96), custom_call_target="tpu_custom_call" | custom-call | tf_op jit(solution)/shard_map/delta_finish/pallas_call | solution.py:205
  328.7 6.1 %fusion.65 = (f32[256]{0:T(256)S(1)}, f32[256]{0:T(256)S(1)}, f32[256,1024]{1,0:T(8,128)}) fusion(bf16[256,1024]{1,0:T(8,128)(2,1)S(1)} %fusion.7, f32[1024]{0:T(1024)S(1)} %bitcast.94, bf16[30,1024]{1,0:T(8,128)(2,1)S(1)} %collective-permute-done.5, f32[1024]{0:T(1024)S(1)} %bitcast.95, f32[1024]{0:T(1024)S(1)} %bitcast.66, f32[1024]{0:T(1024)S(1)} %bitcast.67, ...), kind=kLoop, calls=%fused_computation.121 | loop fusion | flops 48496128 | bytes 1763328 | tf_op jit(solution)/shard_map/reduce_sum | solution.py:390
  334.7 2.4 all-reduce.4
  337.2 4.1 %fusion.12 = f32[256,2048]{1,0:T(8,128)S(1)} fusion(bf16[2048,1024]{1,0:T(8,128)(2,1)} %all-gather.11.cloned.1.call-done, f32[256,1024]{1,0:T(8,128)} %get-tuple-element.21, f32[1024]{0:T(1024)S(1)} %copy-done.8, f32[256]{0:T(256)S(1)} %get-tuple-element.58, f32[256]{0:T(256)S(1)} %get-tuple-element.57), kind=kOutput, calls=%fused_computation.57 | convolution fusion | flops 1075838976 | bytes 7346176 | tf_op jit(solution)/shard_map/dot_general | solution.py:405
  341.3 8.8 %all-gather.5.cloned.1.call-done = bf16[2048,512]{1,0:T(8,128)(2,1)} async-done(((bf16[128,512]{1,0:T(8,128)(2,1)}), bf16[2048,512]{1,0:T(8,128)(2,1)}) %all-gather.5.cloned.1.call-update) | async-done | bytes 2097168 | tf_op jit(solution)/shard_map/all_gather | solution.py:400
  350.1 2.3 fusion
  352.5 2.6 collective-permute-done.6
  (70 shorter events, 16.8 us)
Async XLA Ops:
  6.5 128.9 %copy-start = (bf16[2048,128]{1,0:T(8,128)(2,1)S(1)}, bf16[2048,128]{1,0:T(8,128)(2,1)}, u32[]{:S(2)}) copy-start(bf16[2048,128]{1,0:T(8,128)(2,1)} %param.31) | copy-start | bytes 1572868
  6.5 303.4 %all-gather.9.cloned.1.call-start = ((), (), s32[]{:S(2)}) async-start(), calls=%async_computation.2 | async-start | bytes 4456448 | tf_op jit(solution)/shard_map/all_gather | solution.py:361
  7.3 307.2 %all-gather.7.cloned.1.call-start = ((), (), s32[]{:S(2)}) async-start(), calls=%async_computation.1 | async-start | bytes 4456448 | tf_op jit(solution)/shard_map/all_gather | solution.py:360
  8.0 127.1 %copy-start.1 = (bf16[256,2048]{1,0:T(8,128)(2,1)S(1)}, bf16[256,2048]{1,0:T(8,128)(2,1)}, u32[]{:S(2)}) copy-start(bf16[256,2048]{1,0:T(8,128)(2,1)} %param.20) | copy-start | bytes 3145732
  8.0 329.2 %all-gather.11.cloned.1.call-start = ((), (), s32[]{:S(2)}) async-start(), calls=%async_computation.3 | async-start | bytes 4456448 | tf_op jit(solution)/shard_map/all_gather | solution.py:400
  8.8 341.4 %all-gather.5.cloned.1.call-start = ((), (), s32[]{:S(2)}) async-start(), calls=%async_computation | async-start | bytes 2228224 | tf_op jit(solution)/shard_map/all_gather | solution.py:400
  11.7 123.7 %copy-start.5 = (bf16[128,512]{1,0:T(8,128)(2,1)S(1)}, bf16[128,512]{1,0:T(8,128)(2,1)}, u32[]{:S(2)}) copy-start(bf16[128,512]{1,0:T(8,128)(2,1)} %param.32) | copy-start | bytes 393220
  11.7 123.8 %copy-start.7 = (f32[2048]{0:T(1024)S(1)}, f32[2048]{0:T(1024)}, u32[]{:S(2)}) copy-start(f32[2048]{0:T(1024)} %param.21) | copy-start | bytes 24580
  11.7 123.8 %copy-start.9 = (f32[512]{0:T(512)S(1)}, f32[512]{0:T(512)}, u32[]{:S(2)}) copy-start(f32[512]{0:T(512)} %param.30) | copy-start | bytes 6148
  135.1 1.8 copy-start.4
  135.2 1.8 copy-start.6
  135.2 1.8 copy-start.10
  138.5 3.3 copy-start.12
  141.8 1.6 copy-start.11
  203.0 14.6 %collective-permute-start = (f32[8,128,64]{1,2,0:T(8,128)S(1)}, f32[8,128,64]{1,2,0:T(8,128)S(1)}, u32[]{:S(2)}, u32[]{:S(2)}) collective-permute-start(f32[8,128,64]{1,2,0:T(8,128)S(1)} %bitcast.61), channel_id=1, source_target_pairs={{0,2},{2,4},{4,6},{6,8},{8,10},{10,12},{12,14},{14,16},{16,18},{18... | collective-permute-start | bytes 786440 | tf_op jit(solution)/shard_map/ppermute | solution.py:156
  213.9 80.7 %copy-start.3 = (f32[31,1024]{1,0:T(8,128)S(1)}, f32[31,1024]{1,0:T(8,128)}, u32[]{:S(2)}) copy-start(f32[31,1024]{1,0:T(8,128)} %param.36) | copy-start | bytes 380932
  218.0 11.4 %collective-permute-start.1 = (f32[8,128,64]{1,2,0:T(8,128)S(1)}, f32[8,128,64]{1,2,0:T(8,128)S(1)}, u32[]{:S(2)}, u32[]{:S(2)}) collective-permute-start(f32[8,128,64]{1,2,0:T(8,128)S(1)} %fusion.10), channel_id=1, source_target_pairs={{0,4},{2,6},{4,8},{6,10},{8,12},{10,14},{12,16},{14,18},{16,20},{1... | collective-permute-start | bytes 786440 | tf_op jit(solution)/shard_map/ppermute | solution.py:156
  229.8 45.6 %collective-permute-start.2 = (f32[8,128,64]{1,2,0:T(8,128)S(1)}, f32[8,128,64]{1,2,0:T(8,128)S(1)}, u32[]{:S(2)}, u32[]{:S(2)}) collective-permute-start(f32[8,128,64]{1,2,0:T(8,128)S(1)} %fusion.9), channel_id=1, source_target_pairs={{0,8},{2,10},{4,12},{6,14},{8,16},{10,18},{12,20},{14,22},{16,24},... | collective-permute-start | bytes 786440 | tf_op jit(solution)/shard_map/ppermute | solution.py:156
  275.8 23.6 %collective-permute-start.3 = (f32[8,128,64]{1,2,0:T(8,128)S(1)}, f32[8,128,64]{1,2,0:T(8,128)S(1)}, u32[]{:S(2)}, u32[]{:S(2)}) collective-permute-start(f32[8,128,64]{1,2,0:T(8,128)S(1)} %fusion.8), channel_id=1, source_target_pairs={{0,16},{2,18},{4,20},{6,22},{8,24},{10,26},{12,28},{14,30},{1,17},... | collective-permute-start | bytes 786440 | tf_op jit(solution)/shard_map/ppermute | solution.py:156
  299.9 9.4 %collective-permute-start.4 = (f32[8,64,64]{1,2,0:T(8,128)S(1)}, f32[8,64,64]{1,2,0:T(8,128)S(1)}, u32[]{:S(2)}, u32[]{:S(2)}) collective-permute-start(f32[8,64,64]{1,2,0:T(8,128)S(1)} %fusion.46), channel_id=1, source_target_pairs={{0,2},{2,4},{4,6},{6,8},{8,10},{10,12},{12,14},{14,16},{16,18},{18... | collective-permute-start | bytes 393224 | tf_op jit(solution)/shard_map/ppermute | solution.py:156
  318.3 18.9 %copy-start.8 = (f32[1024]{0:T(1024)S(1)}, f32[1024]{0:T(1024)}, u32[]{:S(2)}) copy-start(f32[1024]{0:T(1024)} %param.37) | copy-start | bytes 12292
  318.4 10.3 %collective-permute-start.5 = (bf16[30,1024]{1,0:T(8,128)(2,1)S(1)}, bf16[30,1024]{1,0:T(8,128)(2,1)S(1)}, u32[]{:S(2)}, u32[]{:S(2)}) collective-permute-start(bf16[30,1024]{1,0:T(8,128)(2,1)S(1)} %slice.316), channel_id=1, source_target_pairs={{0,2},{2,4},{4,6},{6,8},{8,10},{10,12},{12,14},{14,16},{16,18},{18... | collective-permute-start | bytes 184328 | tf_op jit(solution)/shard_map/ppermute | solution.py:156
  337.2 12.9 %copy-start.2 = (bf16[256,512]{1,0:T(8,128)(2,1)S(1)}, bf16[256,512]{1,0:T(8,128)(2,1)}, u32[]{:S(2)}) copy-start(bf16[256,512]{1,0:T(8,128)(2,1)} %delta_finish.1) | copy-start | bytes 786436
  352.5 2.7 collective-permute-start.6
Sparse Core Ops, SparseCore 0:
  10.1 106.6 all-gather.8
  119.6 74.3 all-gather.6
  196.7 81.2 all-gather.10
  280.7 69.3 all-gather.4
